TPU v7x, 256 devices: a whole 4x4x8 slice. The times are simulated.
256 devices in a mesh: sp: 64 (over z, y, core), tp: 4 (over x).
Axes of the slice: x: 4, y: 4, z: 8, core: 2. Of those that a mesh axis runs over, the one named last changes fastest.
Arguments:
- query_one: bfloat16 [16384, 512], P('sp', 'tp'), may hold values from -190 to 190
- query_two: bfloat16 [16384, 512], P('sp', 'tp'), may hold values from -190 to 190
- key_one: bfloat16 [16384, 512], P('sp', 'tp'), may hold values from -10 to 10
- key_two: bfloat16 [16384, 512], P('sp', 'tp'), may hold values from -10 to 10
- values: bfloat16 [16384, 1024], P('sp', 'tp'), may hold values from -6 to 6
- mix_lambda: float32 [8], P('tp'), may hold values from 0.3 to 0.8
- head_gain: float32 [128], replicated, may hold values from 0.1 to 1.9
- stream: bfloat16 [16384, 2048], P('sp', 'tp'), may hold values from -6 to 6
- out_weight: bfloat16 [1024, 2048], P('tp'), may hold values from -0.1875 to 0.1875
- first_gain: float32 [2048], replicated, may hold values from 0.1 to 1.9
- up_weight: bfloat16 [2048, 4096], P('sp', 'tp'), may hold values from -0.125 to 0.125
- down_weight: bfloat16 [4096, 2048], P('tp', 'sp'), may hold values from -0.09375 to 0.09375
- second_gain: float32 [2048], replicated, may hold values from 0.1 to 1.9
Outputs:
- layer_out: bfloat16 [16384, 2048], P(('sp', 'tp'))
All inputs are finite; a program needn't handle non-finite values.
Results may differ from a plain program's by a relative error of at most 0.019.
Values may be sent and summed in bfloat16 or wider, within the bound.
A program may use at most 128 MiB of HBM per device.

v0:
```python
import math

import jax
import jax.numpy as jnp
from jax import lax
from jax.sharding import PartitionSpec as P

alpha_mix = 2.0**0.5


def sent_together(arrays, axis, dim, along):
    both = jnp.concatenate(arrays, axis=along)
    result, at, done = (lax.all_gather(both, axis, axis=dim, tiled=True), 0, [])
    for a in arrays:
        done.append(lax.slice_in_dim(result, at, at + a.shape[along], axis=along))
        at += a.shape[along]
    return tuple(done)


def in_blocks(value, dim, size):
    shape = value.shape
    parts = value.reshape(*shape[:dim], size, shape[dim] // size, *shape[dim + 1 :])
    return jnp.moveaxis(parts, dim, 0)


def sent_and_summed(value, axis, dim):
    size = lax.axis_size(axis)
    parts = lax.all_to_all(in_blocks(value, dim, size), axis, 0, 0, tiled=True)
    return jnp.sum(parts.astype(jnp.float32), axis=0)


def from_everyone(value, axis):
    copies = jnp.broadcast_to(value, (lax.axis_size(axis), *value.shape))
    return lax.all_to_all(copies, axis, split_axis=0, concat_axis=0, tiled=True)


def laid_out(parts, dim):
    shape = list(parts.shape[1:])
    shape[dim] *= parts.shape[0]
    return jnp.moveaxis(parts, 0, dim).reshape(shape)


def gathered_copies(value, axis, dim):
    parts = from_everyone(value, axis)
    return laid_out(parts, dim)


def layer_norm(value, gain):
    centre = jnp.mean(value, axis=-1, keepdims=True)
    spread = jnp.mean(jnp.square(value - centre), axis=-1, keepdims=True)
    return (value - centre) * lax.rsqrt(spread + 1e-05) * gain


def absorb_map(run_max, run_sum, run_acc, queries, keys, vals, scale):
    scores = jnp.einsum("qhd,khd->hqk", queries, keys, preferred_element_type=jnp.float32) * scale
    new_max = jnp.maximum(run_max, jnp.max(scores, axis=-1))
    factor = jnp.exp(run_max - new_max)
    expo = jnp.exp(scores - new_max[..., None])
    run_sum = run_sum * factor + jnp.sum(expo, axis=-1)
    run_acc = run_acc * factor[..., None] + jnp.einsum(
        "hqk,khe->hqe", expo.astype(jnp.bfloat16), vals, preferred_element_type=jnp.float32
    )
    return (new_max, run_sum, run_acc)


def local(
    query_one,
    query_two,
    key_one,
    key_two,
    values,
    mix_lambda,
    head_gain,
    stream,
    out_weight,
    first_gain,
    up_weight,
    down_weight,
    second_gain,
):
    tokens = query_one.shape[0]
    heads_local = mix_lambda.shape[0]
    qk_width = query_one.shape[1] // heads_local
    v_width = values.shape[1] // heads_local
    scale = qk_width ** (-0.5)
    queries_a = query_one.reshape(tokens, heads_local, qk_width)
    queries_b = query_two.reshape(tokens, heads_local, qk_width)
    lowest = jnp.full((heads_local, tokens), -1e30, jnp.float32)
    zero_sum = jnp.zeros((heads_local, tokens), jnp.float32)
    zero_acc = jnp.zeros((heads_local, tokens, v_width), jnp.float32)
    pieces = sent_together((key_one, key_two, values), "sp", 0, 1)
    count = pieces[0].shape[0]
    block = math.gcd(count, 1024)
    nblk = count // block
    keys_a = pieces[0].reshape(nblk, block, heads_local, qk_width)
    keys_b = pieces[1].reshape(nblk, block, heads_local, qk_width)
    vals = pieces[2].reshape(nblk, block, heads_local, v_width)

    def step(carry, inputs):
        max_a, sum_a, acc_a, max_b, sum_b, acc_b = carry
        max_a, sum_a, acc_a = absorb_map(
            max_a, sum_a, acc_a, queries_a, inputs[0], inputs[2], scale
        )
        max_b, sum_b, acc_b = absorb_map(
            max_b, sum_b, acc_b, queries_b, inputs[1], inputs[2], scale
        )
        return ((max_a, sum_a, acc_a, max_b, sum_b, acc_b), None)

    result, _ = lax.scan(
        step, (lowest, zero_sum, zero_acc, lowest, zero_sum, zero_acc), (keys_a, keys_b, vals)
    )
    max_a, sum_a, acc_a, max_b, sum_b, acc_b = result
    mixed = acc_a / sum_a[..., None] - mix_lambda[:, None, None] * acc_b / sum_b[..., None]
    normed = (
        mixed
        * lax.rsqrt(jnp.mean(jnp.square(mixed), axis=-1, keepdims=True) + 1e-05)
        * head_gain
        * 0.8
    )
    attended = jnp.transpose(normed.astype(jnp.bfloat16), (1, 0, 2)).reshape(
        tokens, heads_local * v_width
    )
    tp_index = lax.axis_index("tp")
    own_cols = stream.shape[1]
    col_start = tp_index * own_cols
    share = tokens // lax.axis_size("tp")
    row_start = tp_index * share
    partial_rows = jnp.dot(attended, out_weight, preferred_element_type=jnp.float32)
    own = lax.dynamic_slice_in_dim(partial_rows, col_start, own_cols, 1)
    own = own + alpha_mix * stream.astype(jnp.float32)
    pre_rows = sent_and_summed(
        lax.dynamic_update_slice_in_dim(partial_rows, own, col_start, 1).astype(jnp.bfloat16),
        "tp",
        0,
    )
    hidden_in = gathered_copies(layer_norm(pre_rows, first_gain).astype(jnp.bfloat16), "tp", 0)
    up_full, down_full = (
        lax.all_gather(up_weight, "sp", axis=0, tiled=True),
        lax.all_gather(down_weight, "sp", axis=1, tiled=True),
    )
    upper = jnp.dot(hidden_in, up_full, preferred_element_type=jnp.float32)
    act = jnp.square(jax.nn.relu(upper)).astype(jnp.bfloat16)
    post = sent_and_summed(
        jnp.dot(act, down_full, preferred_element_type=jnp.float32).astype(jnp.bfloat16), "tp", 0
    )
    post = post + alpha_mix * lax.dynamic_slice_in_dim(hidden_in, row_start, share, 0).astype(
        jnp.float32
    )
    return layer_norm(post, second_gain).astype(jnp.bfloat16)


def solution(mesh):
    in_specs = (
        P("sp", "tp"),
        P("sp", "tp"),
        P("sp", "tp"),
        P("sp", "tp"),
        P("sp", "tp"),
        P("tp"),
        P(),
        P("sp", "tp"),
        P("tp", None),
        P(),
        P("sp", "tp"),
        P("tp", "sp"),
        P(),
    )
    out_specs = P(("sp", "tp"), None)
    return jax.shard_map(local, mesh=mesh, in_specs=in_specs, out_specs=out_specs, check_vma=False)
```

profile of v0, /device:TPU:2, one launch (start us, length us, event | category | flops | bytes accessed | tf_op | source)
XLA Modules:
  0.0 383.4 jit_solution(10722259516998093933)
XLA Ops:
  6.5 1.8 pad_maximum_fusion
  11.8 100.6 %all-gather.4.cloned.1.call-done = bf16[16384,512]{1,0:T(8,128)(2,1)} async-done(((bf16[256,512]{1,0:T(8,128)(2,1)}), bf16[16384,512]{1,0:T(8,128)(2,1)}) %all-gather.4.cloned.1.call-update) | async-done | bytes 16777232 | tf_op jit(solution)/shard_map/all_gather | solution.py:13
  112.3 5.8 %fusion.31 = (bf16[16384,128]{1,0:T(8,128)(2,1)}, bf16[16384,128]{1,0:T(8,128)(2,1)}) fusion(bf16[16384,512]{1,0:T(8,128)(2,1)} %all-gather.4.cloned.1.call-done), kind=kLoop, calls=%fused_computation.65 | loop fusion | bytes 16777216 | tf_op jit(solution)/shard_map/slice | solution.py:15
  118.1 14.7 %reshape.78 = bf16[16,1024,2,64]{3,2,1,0:T(2,128)(2,1)} reshape(bf16[16384,128]{1,0:T(8,128)(2,1)} %get-tuple-element.164) | data formatting | bytes 8388608 | tf_op jit(solution)/shard_map/reshape | solution.py:95
  132.8 20.1 %copy.25 = bf16[16,1024,2,64]{1,3,2,0:T(8,128)(2,1)} copy(bf16[16,1024,2,64]{3,2,1,0:T(2,128)(2,1)} %reshape.78) | data formatting | bytes 8388608
  153.0 14.7 %reshape.80 = bf16[16,1024,2,64]{3,2,1,0:T(2,128)(2,1)} reshape(bf16[16384,128]{1,0:T(8,128)(2,1)} %get-tuple-element.163) | data formatting | bytes 8388608 | tf_op jit(solution)/shard_map/reshape | solution.py:96
  167.7 20.3 %copy.27 = bf16[16,1024,2,64]{1,3,2,0:T(8,128)(2,1)} copy(bf16[16,1024,2,64]{3,2,1,0:T(2,128)(2,1)} %reshape.80) | data formatting | bytes 8388608
  187.9 7.1 %slice.13 = bf16[16384,256]{1,0:T(8,128)(2,1)} slice(bf16[16384,512]{1,0:T(8,128)(2,1)} %all-gather.4.cloned.1.call-done), slice={[0:16384], [256:512]} | slice | bytes 16777216 | tf_op jit(solution)/shard_map/slice | solution.py:15
  195.0 12.5 %reshape.79 = bf16[16,1024,2,128]{3,2,1,0:T(2,128)(2,1)} reshape(bf16[16384,256]{1,0:T(8,128)(2,1)} %slice.13) | data formatting | bytes 16777216 | tf_op jit(solution)/shard_map/reshape | solution.py:97
  207.6 104.5 %while.21 = (s32[]{:T(128)}, f32[2,256]{1,0:T(2,128)S(1)}, f32[2,256]{1,0:T(2,128)S(1)}, f32[2,256,128]{2,1,0:T(8,128)S(1)}, f32[2,256]{1,0:T(2,128)S(1)}, /*ind...) while((s32[]{:T(128)}, f32[2,256]{1,0:T(2,128)S(1)}, ...), condition=%wide.region_5.6_spmd.clone, body=%wide.region_0.5_spmd.clone.sunk | while | flops 411440128 | bytes 16450711 | solution.py:109
  207.6 1.5 bitcast_reduce_fusion.4
  209.4 1.4 bitcast_reduce_fusion.5
  211.3 1.4 constant_dynamic-slice_fusion.2
  214.1 1.5 bitcast_reduce_fusion.4
  215.9 1.4 bitcast_reduce_fusion.5
  217.8 1.4 constant_dynamic-slice_fusion.2
  220.6 1.4 bitcast_reduce_fusion.4
  222.5 1.5 bitcast_reduce_fusion.5
  224.3 1.4 constant_dynamic-slice_fusion.2
  227.1 1.5 bitcast_reduce_fusion.4
  229.0 1.4 bitcast_reduce_fusion.5
  230.8 1.4 constant_dynamic-slice_fusion.2
  233.7 1.5 bitcast_reduce_fusion.4
  235.5 1.5 bitcast_reduce_fusion.5
  237.4 1.4 constant_dynamic-slice_fusion.2
  240.2 1.5 bitcast_reduce_fusion.4
  242.0 1.5 bitcast_reduce_fusion.5
  243.9 1.4 constant_dynamic-slice_fusion.2
  246.7 1.4 bitcast_reduce_fusion.4
  248.6 1.5 bitcast_reduce_fusion.5
  250.4 1.4 constant_dynamic-slice_fusion.2
  253.3 1.5 bitcast_reduce_fusion.4
  255.1 1.5 bitcast_reduce_fusion.5
  257.0 1.4 constant_dynamic-slice_fusion.2
  259.8 1.5 bitcast_reduce_fusion.4
  261.6 1.4 bitcast_reduce_fusion.5
  263.5 1.4 constant_dynamic-slice_fusion.2
  266.3 1.5 bitcast_reduce_fusion.4
  268.2 1.5 bitcast_reduce_fusion.5
  270.0 1.4 constant_dynamic-slice_fusion.2
  272.9 1.5 bitcast_reduce_fusion.4
  274.7 1.4 bitcast_reduce_fusion.5
  276.6 1.4 constant_dynamic-slice_fusion.2
  279.4 1.5 bitcast_reduce_fusion.4
  281.2 1.5 bitcast_reduce_fusion.5
  283.1 1.4 constant_dynamic-slice_fusion.2
  285.9 1.5 bitcast_reduce_fusion.4
  287.8 1.5 bitcast_reduce_fusion.5
  289.6 1.4 constant_dynamic-slice_fusion.2
  292.5 1.5 bitcast_reduce_fusion.4
  294.3 1.4 bitcast_reduce_fusion.5
  296.1 1.4 constant_dynamic-slice_fusion.2
  299.0 1.5 bitcast_reduce_fusion.4
  300.8 1.5 bitcast_reduce_fusion.5
  302.7 1.4 constant_dynamic-slice_fusion.2
  305.5 1.5 bitcast_reduce_fusion.4
  307.4 1.5 bitcast_reduce_fusion.5
  309.2 1.4 constant_dynamic-slice_fusion.2
  313.6 18.6 %all_to_all.15 = bf16[4,64,2048]{2,1,0:T(8,128)(2,1)S(1)} all-to-all(bf16[4,64,2048]{2,1,0:T(8,128)(2,1)S(1)} %bitcast.73), channel_id=1, replica_groups=mesh['sp'=64,'tp'=4] {'tp'}, dimensions={0} | all-to-all | bytes 2097152 | tf_op jit(solution)/shard_map/all_to_all | solution.py:28
  334.0 4.9 %all-to-all-start.1 = ((bf16[4,64,2048]{2,1,0:T(8,128)(2,1)}), bf16[4,64,2048]{2,1,0:T(8,128)(2,1)S(1)}, u32[]{:S(2)}, u32[]{:S(2)}) async-start(bf16[4,64,2048]{2,1,0:T(8,128)(2,1)} %broadcast_in_dim.15), calls=%async_computation.1 | async-start | bytes 2097152 | tf_op jit(solution)/shard_map/all_to_all | solution.py:34
  338.9 12.8 %all-to-all-done.1 = bf16[4,64,2048]{2,1,0:T(8,128)(2,1)S(1)} async-done(((bf16[4,64,2048]{2,1,0:T(8,128)(2,1)}), bf16[4,64,2048]{2,1,0:T(8,128)(2,1)S(1)}, u32[]{:S(2)}, u32[]{:S(2)}) %all-to-all-start.1) | async-done | bytes 1048608 | tf_op jit(solution)/shard_map/all_to_all | solution.py:34
  351.7 6.8 %convolution_convert_fusion = bf16[256,2048]{1,0:T(8,128)(2,1)} fusion(bf16[1024,2048]{0,1:T(8,128)(2,1)} %all-gather.8.cloned.1.call-done, bf16[256,2048]{1,0:T(8,128)(2,1)S(1)} %bitcast.74, bf16[2048,1024]{1,0:T(8,128)(2,1)} %all-gather.6.cloned.1.call-done), kind=kOutput, calls=%fused_computation.42 | convolution fusion | flops 2148794368 | bytes 10485760 | tf_op jit(solution)/shard_map/dot_general | solution.py:144
  358.5 4.9 %all-to-all-start.2 = ((bf16[4,64,2048]{2,1,0:T(8,128)(2,1)}), bf16[4,64,2048]{2,1,0:T(8,128)(2,1)S(1)}, u32[]{:S(2)}, u32[]{:S(2)}) async-start(bf16[4,64,2048]{2,1,0:T(8,128)(2,1)} %bitcast.80), calls=%async_computation.2 | async-start | bytes 2097152 | tf_op jit(solution)/shard_map/all_to_all | solution.py:28
  363.5 12.0 %all-to-all-done.2 = bf16[4,64,2048]{2,1,0:T(8,128)(2,1)S(1)} async-done(((bf16[4,64,2048]{2,1,0:T(8,128)(2,1)}), bf16[4,64,2048]{2,1,0:T(8,128)(2,1)S(1)}, u32[]{:S(2)}, u32[]{:S(2)}) %all-to-all-start.2) | async-done | bytes 1048608 | tf_op jit(solution)/shard_map/all_to_all | solution.py:28
  (192 shorter events, 42.3 us)
Async XLA Ops:
  6.5 306.1 %copy-start = (bf16[256,2048]{1,0:T(8,128)(2,1)S(1)}, bf16[256,2048]{1,0:T(8,128)(2,1)}, u32[]{:S(2)}) copy-start(bf16[256,2048]{1,0:T(8,128)(2,1)} %param.23) | copy-start | bytes 3145732
  6.5 105.8 %all-gather.4.cloned.1.call-start = ((), (), s32[]{:S(2)}) async-start(), calls=%async_computation.3 | async-start | bytes 17039360 | tf_op jit(solution)/shard_map/all_gather | solution.py:13
  8.3 330.6 %all-gather.6.cloned.1.call-start = ((), (), s32[]{:S(2)}) async-start(), calls=%async_computation.4 | async-start | bytes 4259840 | tf_op jit(solution)/shard_map/all_gather | solution.py:138
  9.1 329.8 %all-gather.8.cloned.1.call-start = ((), (), s32[]{:S(2)}) async-start(), calls=%async_computation.5 | async-start | bytes 4259840 | tf_op jit(solution)/shard_map/all_gather | solution.py:139
  207.6 104.7 %copy-start.5 = (f32[2]{0:T(128)S(1)}, f32[2]{0:T(128)}, u32[]{:S(2)}) copy-start(f32[2]{0:T(128)} %param.20) | copy-start | bytes 28
  207.6 104.9 %copy-start.4 = (f32[128]{0:T(128)S(1)}, f32[128]{0:T(128)}, u32[]{:S(2)}) copy-start(f32[128]{0:T(128)} %param.21) | copy-start | bytes 1540
  312.3 1.0 copy-start.1
  313.5 19.2 %copy-start.2 = (f32[2048]{0:T(1024)S(1)}, f32[2048]{0:T(1024)}, u32[]{:S(2)}) copy-start(f32[2048]{0:T(1024)} %param.24) | copy-start | bytes 24580
  334.0 17.8 %all-to-all-start.1 = ((bf16[4,64,2048]{2,1,0:T(8,128)(2,1)}), bf16[4,64,2048]{2,1,0:T(8,128)(2,1)S(1)}, u32[]{:S(2)}, u32[]{:S(2)}) async-start(bf16[4,64,2048]{2,1,0:T(8,128)(2,1)} %broadcast_in_dim.15), calls=%async_computation.1 | async-start | bytes 2097152 | tf_op jit(solution)/shard_map/all_to_all | solution.py:34
  358.5 16.9 %all-to-all-start.2 = ((bf16[4,64,2048]{2,1,0:T(8,128)(2,1)}), bf16[4,64,2048]{2,1,0:T(8,128)(2,1)S(1)}, u32[]{:S(2)}, u32[]{:S(2)}) async-start(bf16[4,64,2048]{2,1,0:T(8,128)(2,1)} %bitcast.80), calls=%async_computation.2 | async-start | bytes 2097152 | tf_op jit(solution)/shard_map/all_to_all | solution.py:28
  363.5 12.6 %copy-start.3 = (f32[2048]{0:T(1024)S(1)}, f32[2048]{0:T(1024)}, u32[]{:S(2)}) copy-start(f32[2048]{0:T(1024)} %param.27) | copy-start | bytes 24580
Sparse Core Ops, SparseCore 0:
  10.1 102.1 all-gather.3
  115.1 76.2 all-gather.5
  194.1 76.0 all-gather.7
where the time goes:
time: 388 us; the launch traced here: 383 us
  waiting for transfers between devices  127 us (33%)
  local copies, waits for them, and re-layouts  121 us (31%)
  matrix products  75.8 us (20%)
  blocking collectives  18.6 us (5%)
  other arithmetic  16.5 us (4%)
  between operations  13.3 us (3%)
  starting transfers between devices  9.97 us (3%)
    all_gather x1, waiting for transfers between devices, sent_together(): result, at, done = (lax.all_gather(both, axis, axis=dim, tiled=True), 0, [])  101 us
    dot_general x32, matrix products, absorb_map(): jnp.einsum('qhd,khd->hqk', queries, keys, preferred_element_type=jnp.floa...  46.5 us
    unnamed x16, local copies, waits for them, and re-layouts  42.5 us
    dynamic_slice x16, local copies, waits for them, and re-layouts, local(): lax.scan(step, (lowest, zero_sum, zero_acc, lowest, zero_sum, zero_acc),...  22.6 us
    dot_general x32, matrix products, absorb_map(): jnp.einsum('hqk,khe->hqe', expo.astype(jnp.bfloat16), vals, preferred_ele...  22 us
    all_to_all x1, blocking collectives, sent_and_summed(): parts = lax.all_to_all(in_blocks(value, dim, size), axis, 0, 0, tiled=True)  18.6 us
    reshape x1, local copies, waits for them, and re-layouts, local(): keys_a = pieces[0].reshape(nblk, block, heads_local, qk_width)  14.7 us
    reshape x1, local copies, waits for them, and re-layouts, local(): keys_b = pieces[1].reshape(nblk, block, heads_local, qk_width)  14.7 us
  transfers between devices with their start and end apart: 5, of which 3 were waited for; matrix products, arithmetic and copies ran while one was open for 53% of the time, Pallas kernels for 0%

commit v1 on v0

v1 whole, which is shorter than its diff:
```python
import functools

import jax
import jax.numpy as jnp
from jax import lax
from jax.experimental import pallas as pl
from jax.experimental.pallas import tpu as pltpu
from jax.sharding import PartitionSpec as P

MESH = pl.DeviceIdType.MESH
NZ, NY, NX = 8, 4, 4
ALPHA = 2.0**0.5
LOG2E = 1.4426950408889634
CEXP = LOG2E * 64 ** (-0.5)
LOW = -1e30
TOK = 256
SUB = 64
NT = (((1,), (1,)), ((), ()))


def layer_norm(value, gain):
    centre = jnp.mean(value, axis=-1, keepdims=True)
    spread = jnp.mean(jnp.square(value - centre), axis=-1, keepdims=True)
    return (value - centre) * lax.rsqrt(spread + 1e-05) * gain


def attention_kernel(
    lam_ref, q1_ref, q2_ref, k1_ref, k2_ref, v_ref, gain_ref, stream_ref,
    att_out, str_out,
    kvsrc, qsrc, kvbuf, qbuf, acc, mbuf, lbuf, osend, ssend, orecv, srecv, attown, attbuf, strbuf,
    snd, kv_rcv, q_rcv, o_rcv, s_rcv, str_rcv, att_rcv,
):
    sp = lax.axis_index("sp")
    x = lax.axis_index("tp")
    c = lax.rem(sp, 2)
    y = lax.rem(sp // 2, NY)
    z = sp // (2 * NY)

    def dev(dz=0, dy=0, core=None, dx=0):
        zz = lax.rem(z + (dz + NZ), NZ)
        yy = lax.rem(y + (dy + NY), NY)
        cc = c if core is None else core
        return {"sp": (zz * NY + yy) * 2 + cc, "tp": lax.rem(x + (dx + NX), NX)}

    count = [0]
    started = []

    def send(src, dst, rcv, to):
        k = count[0]
        count[0] += 1
        cp = pltpu.make_async_remote_copy(
            src_ref=src, dst_ref=dst, send_sem=snd.at[k], recv_sem=rcv, device_id=to, device_id_type=MESH
        )
        cp.start()
        started.append(cp)

    def arrived(dst, rcv):
        pltpu.make_async_remote_copy(
            src_ref=dst, dst_ref=dst, send_sem=snd.at[0], recv_sem=rcv, device_id=dev(core=1 - c),
            device_id_type=MESH,
        ).wait_recv()

    barrier = pltpu.get_barrier_semaphore()
    partners = [dev(core=1 - c), dev(dy=2)]
    for core in (0, 1):
        partners += [dev(dz=1, core=core), dev(dz=-1, core=core), dev(dy=1, core=core), dev(dy=-1, core=core)]
        partners += [dev(dx=d, core=core) for d in (1, 2, 3)]
    for p in partners:
        pl.semaphore_signal(barrier, inc=1, device_id=p, device_id_type=MESH)

    lane = lax.broadcasted_iota(jnp.int32, (TOK, 128), 1)
    low_half = lane < 64

    def by_head(one_ref, two_ref):
        one, two = one_ref[...].astype(jnp.float32), two_ref[...].astype(jnp.float32)
        first = jnp.where(low_half, one, pltpu.roll(two, 64, 1))
        second = jnp.where(low_half, pltpu.roll(one, 64, 1), two)
        return first.astype(jnp.bfloat16), second.astype(jnp.bfloat16)

    for h, part in enumerate(by_head(q1_ref, q2_ref)):
        qsrc[h] = part
    vt = v_ref[...].astype(jnp.float32).T.astype(jnp.bfloat16)
    for h, part in enumerate(by_head(k1_ref, k2_ref)):
        kvsrc[h, 0:256, :] = part
        kvsrc[h, 256:384, :] = vt[128 * h : 128 * h + 128, 0:128]
        kvsrc[h, 384:512, :] = vt[128 * h : 128 * h + 128, 128:256]
    kvbuf[0, c] = kvsrc[c]
    qbuf[0, c] = qsrc[c]
    strbuf[x] = stream_ref[pl.ds(pl.multiple_of(x * SUB, SUB), SUB), :]
    mbuf[...] = jnp.full(mbuf.shape, LOW, jnp.float32)
    lbuf[...] = jnp.zeros(lbuf.shape, jnp.float32)

    def clear(i, carry):
        acc[i] = jnp.zeros(acc.shape[1:], jnp.float32)
        return carry

    lax.fori_loop(0, acc.shape[0], clear, 0)
    pl.semaphore_wait(barrier, len(partners))

    sibling = dev(core=1 - c)
    send(qsrc.at[1 - c], qbuf.at[0, c], q_rcv.at[0, c], sibling)
    send(kvsrc.at[1 - c], kvbuf.at[0, c], kv_rcv.at[0, c], sibling)
    for h in (0, 1):
        send(kvsrc.at[h], kvbuf.at[1, c], kv_rcv.at[1, c], dev(dz=1, core=h))
        send(kvsrc.at[h], kvbuf.at[2, c], kv_rcv.at[2, c], dev(dz=-1, core=h))
        send(qsrc.at[h], qbuf.at[1, c], q_rcv.at[1, c], dev(dy=1, core=h))
        send(qsrc.at[h], qbuf.at[2, c], q_rcv.at[2, c], dev(dy=-1, core=h))
    for dx in (1, 2, 3):
        rows = pl.ds(pl.multiple_of(lax.rem(x + dx, NX) * SUB, SUB), SUB)
        send(stream_ref.at[rows, :], strbuf.at[x], str_rcv.at[dx - 1], dev(dx=dx))

    def take_kv(slot):
        for cc in (0, 1):
            arrived(kvbuf.at[slot, cc], kv_rcv.at[slot, cc])
            step = 1 if slot % 2 else -1
            if slot <= 4:
                send(kvbuf.at[slot, cc], kvbuf.at[slot + 2, cc], kv_rcv.at[slot + 2, cc], dev(dz=step))
            elif (slot, cc) in ((5, 0), (6, 1)):
                send(kvbuf.at[slot, cc], kvbuf.at[7, cc], kv_rcv.at[7, cc], dev(dz=step))

    def take_q(slot):
        for cc in (0, 1):
            arrived(qbuf.at[slot, cc], q_rcv.at[slot, cc])
            if (slot, cc) in ((1, 0), (2, 1)):
                send(qbuf.at[slot, cc], qbuf.at[3, cc], q_rcv.at[3, cc], dev(dy=1 if slot == 1 else -1))

    row_lane = lax.broadcasted_iota(jnp.int32, (1, 128), 1)
    masks = [jnp.where(row_lane < 64, 1.0, 0.0).astype(jnp.bfloat16), jnp.where(row_lane < 64, 0.0, 1.0).astype(jnp.bfloat16)]

    def unit(kvs, qs):
        keys = jnp.concatenate([kvbuf[kvs, cc, 0:256, :] for cc in (0, 1)], axis=0)
        vals = jnp.concatenate(
            [kvbuf[kvs, cc, 256 + 128 * i : 384 + 128 * i, :] for cc in (0, 1) for i in (0, 1)], axis=1
        )
        for cc in (0, 1):
            for mp in (0, 1):
                at = qs * 4 + (2 * cc + mp)
                query = qbuf[qs, cc] * masks[mp]
                scores = lax.dot_general(keys, query, NT, preferred_element_type=jnp.float32)
                old = mbuf[at]
                new = jnp.maximum(old, jnp.max(scores, axis=0, keepdims=True))
                factor = jnp.exp2((old - new) * CEXP)
                expo = jnp.exp2((scores - new) * CEXP)
                mbuf[at] = new
                lbuf[at] = lbuf[at] * factor + jnp.sum(expo, axis=0, keepdims=True)
                acc[at] = acc[at] * factor + jnp.dot(
                    vals, expo.astype(jnp.bfloat16), preferred_element_type=jnp.float32
                )

    def process(kv_lo, kv_n, q_lo, q_n):
        def trip(i, carry):
            unit(kv_lo + i // q_n, q_lo + lax.rem(i, q_n))
            return carry

        lax.fori_loop(0, kv_n * q_n, trip, 0)

    def finish(qs):
        for cc in (0, 1):
            for mp in (0, 1):
                at = qs * 4 + 2 * cc + mp
                osend[qs - 1, 2 * cc + mp] = (acc[at] / lbuf[at]).astype(jnp.bfloat16)
        for cc in (0, 1):
            for mp in (0, 1):
                at = qs * 4 + 2 * cc + mp
                ssend[qs - 1, 2 * cc + mp] = mbuf[at]
                ssend[qs - 1, 4 + 2 * cc + mp] = lbuf[at]
        to, land = {1: (dev(dy=-1), 1), 2: (dev(dy=1), 0), 3: (dev(dy=2), 2)}[qs]
        send(osend.at[qs - 1], orecv.at[land], o_rcv.at[land], to)
        send(ssend.at[qs - 1], srecv.at[land], s_rcv.at[land], to)

    arrived(qbuf.at[0, 1 - c], q_rcv.at[0, 1 - c])
    arrived(kvbuf.at[0, 1 - c], kv_rcv.at[0, 1 - c])
    process(0, 1, 0, 1)
    take_q(1)
    take_q(2)
    process(0, 1, 1, 2)
    take_kv(1)
    take_kv(2)
    process(1, 2, 0, 3)
    take_q(3)
    process(0, 3, 3, 1)
    take_kv(3)
    take_kv(4)
    process(3, 2, 0, 4)
    take_kv(5)
    take_kv(6)
    take_kv(7)
    for qs in (3, 1, 2):
        process(5, 3, qs, 1)
        finish(qs)
    process(5, 3, 0, 1)

    for j in (2, 1, 0):
        arrived(orecv.at[j], o_rcv.at[j])
        arrived(srecv.at[j], s_rcv.at[j])
    lam = lam_ref[c]
    gain = gain_ref[...] * 0.8
    for cc in (0, 1):
        maps = []
        for mp in (0, 1):
            i = 2 * cc + mp
            ms = [mbuf[i]] + [srecv[j, i] for j in range(3)]
            ls = [lbuf[i]] + [srecv[j, 4 + i] for j in range(3)]
            top = functools.reduce(jnp.maximum, ms)
            ws = [jnp.exp2((m - top) * CEXP) for m in ms]
            total = ws[0] * ls[0]
            out = acc[i] * ws[0]
            for j in range(3):
                w = ws[j + 1] * ls[j + 1]
                total = total + w
                out = out + orecv[j, i].astype(jnp.float32) * w
            maps.append(out / total)
        mixed = maps[0] - lam * maps[1]
        inv = lax.rsqrt(jnp.mean(mixed * mixed, axis=0, keepdims=True) + 1e-5)
        attown[cc] = ((mixed * inv).T * gain).astype(jnp.bfloat16)

    head = 2 * x + c
    for dx in range(NX):
        for dc in (0, 1):
            if dx == 0 and dc == 0:
                continue
            cc = c if dc == 0 else 1 - c
            rows = pl.ds(pl.multiple_of(lax.rem(x + dx, NX) * SUB, SUB), SUB)
            send(attown.at[cc, rows, :], attbuf.at[head], att_rcv.at[2 * dx + dc - 1], dev(dx=dx, core=cc))
    attbuf[head] = attown[c, pl.ds(pl.multiple_of(x * SUB, SUB), SUB), :]
    for dx in (1, 2, 3):
        src = lax.rem(x + (NX - dx), NX)
        arrived(strbuf.at[src], str_rcv.at[dx - 1])
    for dx in range(NX):
        for dc in (0, 1):
            if dx == 0 and dc == 0:
                continue
            cc = c if dc == 0 else 1 - c
            src = 2 * lax.rem(x + (NX - dx), NX) + cc
            arrived(attbuf.at[src], att_rcv.at[2 * dx + dc - 1])
    for h in range(8):
        att_out[:, 128 * h : 128 * h + 128] = attbuf[h]
    for i in range(NX):
        str_out[:, 512 * i : 512 * i + 512] = strbuf[i]
    for cp in started:
        cp.wait_send()


def attention(lam, q1, q2, k1, k2, v, gain, stream):
    bf, f32 = jnp.bfloat16, jnp.float32
    vm = pl.BlockSpec(memory_space=pltpu.VMEM)
    dma = pltpu.SemaphoreType.DMA
    return pl.pallas_call(
        attention_kernel,
        out_shape=(jax.ShapeDtypeStruct((SUB, 1024), bf), jax.ShapeDtypeStruct((SUB, 2048), bf)),
        in_specs=[pl.BlockSpec(memory_space=pltpu.SMEM)] + [vm] * 7,
        out_specs=(vm, vm),
        scratch_shapes=[
            pltpu.VMEM((2, 512, 128), bf),
            pltpu.VMEM((2, 256, 128), bf),
            pltpu.VMEM((8, 2, 512, 128), bf),
            pltpu.VMEM((4, 2, 256, 128), bf),
            pltpu.VMEM((16, 128, 256), f32),
            pltpu.VMEM((16, 1, 256), f32),
            pltpu.VMEM((16, 1, 256), f32),
            pltpu.VMEM((3, 4, 128, 256), bf),
            pltpu.VMEM((3, 8, 1, 256), f32),
            pltpu.VMEM((3, 4, 128, 256), bf),
            pltpu.VMEM((3, 8, 1, 256), f32),
            pltpu.VMEM((2, 256, 128), bf),
            pltpu.VMEM((8, SUB, 128), bf),
            pltpu.VMEM((NX, SUB, 512), bf),
            dma((48,)),
            dma((8, 2)),
            dma((4, 2)),
            dma((3,)),
            dma((3,)),
            dma((3,)),
            dma((7,)),
        ],
        compiler_params=pltpu.CompilerParams(
            collective_id=0, has_side_effects=True, vmem_limit_bytes=40 * 1024 * 1024
        ),
        cost_estimate=pl.CostEstimate(flops=20_000_000_000, bytes_accessed=4_000_000, transcendentals=17_000_000),
        name="attention",
    )(lam, q1, q2, k1, k2, v, gain.reshape(1, 128), stream)


def in_blocks(value, dim, size):
    shape = value.shape
    parts = value.reshape(*shape[:dim], size, shape[dim] // size, *shape[dim + 1 :])
    return jnp.moveaxis(parts, dim, 0)


def local(
    query_one, query_two, key_one, key_two, values, mix_lambda, head_gain, stream, out_weight, first_gain,
    up_weight, down_weight, second_gain,
):
    bf, f32 = jnp.bfloat16, jnp.float32
    both = jnp.concatenate([up_weight, down_weight.T], axis=0)
    weights = lax.all_gather(both, "sp", axis=0, tiled=False)
    up_full = weights[:, 0:32, :].reshape(2048, 1024)
    down_t = weights[:, 32:64, :].reshape(2048, 1024)
    out_full = lax.all_gather(out_weight, "tp", axis=0, tiled=True)
    attended, rows = attention(mix_lambda, query_one, query_two, key_one, key_two, values, head_gain, stream)
    pre = ALPHA * rows.astype(f32) + jnp.dot(attended, out_full, preferred_element_type=f32)
    own = layer_norm(pre, first_gain).astype(bf)
    hidden = lax.all_to_all(jnp.broadcast_to(own, (NX, *own.shape)), "tp", 0, 0, tiled=True).reshape(TOK, 2048)
    upper = jnp.dot(hidden, up_full, preferred_element_type=f32)
    act = jnp.square(jax.nn.relu(upper)).astype(bf)
    part = lax.dot_general(act, down_t, NT, preferred_element_type=f32).astype(bf)
    parts = lax.all_to_all(part.reshape(NX, SUB, 2048), "tp", 0, 0, tiled=True)
    post = jnp.sum(parts.astype(f32), axis=0) + ALPHA * own.astype(f32)
    return layer_norm(post, second_gain).astype(bf)


def solution(mesh):
    in_specs = (
        P("sp", "tp"), P("sp", "tp"), P("sp", "tp"), P("sp", "tp"), P("sp", "tp"), P("tp"), P(), P("sp", "tp"),
        P("tp", None), P(), P("sp", "tp"), P("tp", "sp"), P(),
    )
    return jax.shard_map(
        local, mesh=mesh, in_specs=in_specs, out_specs=P(("sp", "tp"), None), check_vma=False
    )
```

time: 388 us -> 190 us (0.49)
  local copies, waits for them, and re-layouts: 121 us -> 13.9 us
  waiting for transfers between devices: 127 us -> 42.9 us
  Pallas kernels: 0 us -> 81.7 us
  matrix products: 75.8 us -> 8.95 us
  other arithmetic: 16.5 us -> 3.64 us
  starting transfers between devices: 9.97 us -> 5.32 us
    pallas_call x0 -> x1, Pallas kernels: none -> 81.7 us  [attention(): pl.pallas_call(attention_kernel, out_shape=(jax.ShapeDtypeStruct((SUB, 10...]
    dot_general x66 -> x2, matrix products: 75.8 us -> 8.95 us  [the longest x1 5.81 us: local(): lax.dot_general(act, down_t, NT, preferred_element_type=f32).astype(bf)]
    all_gather x3 -> x2, waiting for transfers between devices: 101 us -> 42.1 us  [the longest x1 42.1 us: local(): weights = lax.all_gather(both, 'sp', axis=0, tiled=False)]
    reshape x3 -> x0, local copies, waits for them, and re-layouts: 41.9 us -> none  [the longest x1 14.7 us: local(): keys_a = pieces[0].reshape(nblk, block, heads_local, qk_width)]
    unnamed x16 -> x20, local copies, waits for them, and re-layouts: 42.5 us -> 6.53 us
    all_to_all x2 -> x1, waiting for transfers between devices: 24.8 us -> 0.01 us  [local(): lax.all_to_all(jnp.broadcast_to(own, (NX, *own.shape)), 'tp', 0, 0, tiled...]
    dynamic_slice x16 -> x0, local copies, waits for them, and re-layouts: 22.6 us -> none  [local(): lax.scan(step, (lowest, zero_sum, zero_acc, lowest, zero_sum, zero_acc),...]
    reduce_sum x34 -> x1, other arithmetic: 11.9 us -> 0.16 us  [local(): post = jnp.sum(parts.astype(f32), axis=0) + ALPHA * own.astype(f32)]
  transfers between devices with their start and end apart: 5 -> 3, of which waited for: 3 -> 1; matrix products, arithmetic and copies ran while one was open for 53% -> 7% of each run, Pallas kernels for 0% -> 43%
where the time goes in v1:
time: 190 us; the launch traced here: 188 us
  Pallas kernels  81.7 us (43%)
  waiting for transfers between devices  42.9 us (23%)
  blocking collectives  18.7 us (10%)
  local copies, waits for them, and re-layouts  13.9 us (7%)
  between operations  13.5 us (7%)
  matrix products  8.95 us (5%)
  starting transfers between devices  5.32 us (3%)
  other arithmetic  3.64 us (2%)
    pallas_call x1, Pallas kernels, attention(): pl.pallas_call(attention_kernel, out_shape=(jax.ShapeDtypeStruct((SUB, 10...  81.7 us
    all_gather x1, waiting for transfers between devices, local(): weights = lax.all_gather(both, 'sp', axis=0, tiled=False)  42.1 us
    all_to_all x1, blocking collectives, local(): parts = lax.all_to_all(part.reshape(NX, SUB, 2048), 'tp', 0, 0, tiled=True)  18.7 us
    unnamed x20, local copies, waits for them, and re-layouts  6.53 us
    slice x1, local copies, waits for them, and re-layouts, local(): up_full = weights[:, 0:32, :].reshape(2048, 1024)  6.24 us
    dot_general x1, matrix products, local(): lax.dot_general(act, down_t, NT, preferred_element_type=f32).astype(bf)  5.81 us
    all_to_all x1, starting transfers between devices, local(): lax.all_to_all(jnp.broadcast_to(own, (NX, *own.shape)), 'tp', 0, 0, tiled...  5.27 us
  transfers between devices with their start and end apart: 3, of which 1 were waited for; matrix products, arithmetic and copies ran while one was open for 7% of the time, Pallas kernels for 43%

profile of v1, /device:TPU:2, one launch (start us, length us, event | category | flops | bytes accessed | tf_op | source)
XLA Modules:
  0.0 188.5 jit_solution(1686061971307324272)
XLA Ops:
  6.5 0.0 all-gather.4.cloned.1.call-start
  6.5 0.7 all-gather.4.cloned.1.call-update
  7.3 0.0 all-gather.6.cloned.1.call-start
  7.3 1.5 pad_maximum_fusion
  8.8 0.0 all-gather.6.cloned.1.call-update
  8.9 0.0 copy-start
  8.9 0.9 copy-done
  9.8 0.0 copy-start.1
  9.8 0.9 copy-done.1
  10.7 0.0 copy-start.2
  10.7 0.8 copy-done.2
  11.6 0.0 copy-start.3
  11.6 0.8 copy-done.3
  12.4 0.0 copy-start.4
  12.4 0.8 copy-done.4
  13.2 0.0 copy-start.5
  13.2 0.8 copy-done.5
  14.1 0.0 copy-start.6
  14.1 0.7 copy-done.6
  14.7 0.0 copy-start.7
  14.7 0.7 copy-done.7
  15.4 81.7 %attention.1 = (bf16[64,1024]{1,0:T(8,128)(2,1)S(1)}, bf16[64,2048]{1,0:T(8,128)(2,1)S(1)}) custom-call(f32[2]{0:T(128)S(1)} %copy-done.6, bf16[256,128]{1,0:T(8,128)(2,1)S(1)} %copy-done.2, bf16[256,128]{1,0:T(8,128)(2,1)S(1)} %copy-done.3, bf16[256,128]{1,0:T(8,128)(2,1)S(1)} %copy-done.4, bf16[256,128]{1,0:T(8,128)(2,1)S(1)} %copy-done.5, ...), custom_call_target="tpu_custom_call" | custom-call | flops 20000000000 | bytes 4000000 | tf_op jit(solution)/shard_map/attention/pallas_call | solution.py:248
  97.1 0.0 copy-start.8
  97.1 0.0 all-gather.4.cloned.1.call-done
  97.1 3.1 %fusion.6 = (f32[64]{0:T(128)S(1)}, f32[64,2048]{1,0:T(8,128)S(1)}) fusion(bf16[64,1024]{1,0:T(8,128)(2,1)S(1)} %get-tuple-element.8, bf16[1024,2048]{1,0:T(8,128)(2,1)} %all-gather.4.cloned.1.call-done, bf16[64,2048]{1,0:T(8,128)(2,1)S(1)} %get-tuple-element.7), kind=kOutput, calls=%fused_computation.20 | convolution fusion | flops 268959680 | bytes 5112064 | tf_op jit(solution)/shard_map/dot_general | solution.py:301
  100.3 0.2 multiply_reduce_fusion.1
  100.5 0.0 copy-done.8
  100.5 0.1 multiply_convert_fusion.1
  100.7 1.1 broadcast_in_dim.2
  101.8 5.3 %all-to-all-start = ((bf16[4,64,2048]{2,1,0:T(8,128)(2,1)}), bf16[4,64,2048]{2,1,0:T(8,128)(2,1)S(1)}, u32[]{:S(2)}, u32[]{:S(2)}) async-start(bf16[4,64,2048]{2,1,0:T(8,128)(2,1)} %broadcast_in_dim.2), calls=%async_computation | async-start | bytes 2097152 | tf_op jit(solution)/shard_map/all_to_all | solution.py:303
  107.1 42.1 %all-gather.6.cloned.1.call-done = bf16[4096,1024]{1,0:T(8,128)(2,1)} async-done(((bf16[64,1024]{1,0:T(8,128)(2,1)}), bf16[4096,1024]{1,0:T(8,128)(2,1)}) %all-gather.6.cloned.1.call-update) | async-done | bytes 8388624 | tf_op jit(solution)/shard_map/all_gather | solution.py:296
  149.2 6.2 %fusion.5 = (bf16[64,32,1024]{2,1,0:T(8,128)(2,1)}, bf16[64,32,1024]{2,1,0:T(8,128)(2,1)}) fusion(bf16[64,64,1024]{2,1,0:T(8,128)(2,1)} %bitcast.13), kind=kLoop, calls=%fused_computation.19 | loop fusion | bytes 16777216 | tf_op jit(solution)/shard_map/slice | solution.py:297
  155.4 0.0 all-to-all-done
  155.4 5.8 %convolution_convert_fusion = bf16[256,2048]{1,0:T(8,128)(2,1)S(1)} fusion(bf16[2048,1024]{1,0:T(8,128)(2,1)} %bitcast.15, bf16[256,2048]{1,0:T(8,128)(2,1)S(1)} %bitcast.16, bf16[2048,1024]{1,0:T(8,128)(2,1)} %bitcast.14), kind=kOutput, calls=%fused_computation | convolution fusion | flops 2148794368 | bytes 10485760 | tf_op jit(solution)/shard_map/dot_general | solution.py:306
  161.2 0.0 copy-start.9
  161.3 18.7 %all_to_all.10 = bf16[4,64,2048]{2,1,0:T(8,128)(2,1)S(1)} all-to-all(bf16[4,64,2048]{2,1,0:T(8,128)(2,1)S(1)} %bitcast.17), channel_id=1, replica_groups=mesh['sp'=64,'tp'=4] {'tp'}, dimensions={0} | all-to-all | bytes 2097152 | tf_op jit(solution)/shard_map/all_to_all | solution.py:307
  179.9 0.2 convert_reduce_fusion
  180.1 0.3 fusion.3
  180.3 0.3 multiply_reduce_fusion
  180.7 0.0 copy-done.9
  180.7 1.0 multiply_convert_fusion
  (4 shorter events, 0.0 us)
Async XLA Ops:
  6.5 90.6 %all-gather.4.cloned.1.call-start = ((), (), s32[]{:S(2)}) async-start(), calls=%async_computation.2 | async-start | bytes 5242880 | tf_op jit(solution)/shard_map/all_gather | solution.py:299
  7.3 141.9 %all-gather.6.cloned.1.call-start = ((), (), s32[]{:S(2)}) async-start(), calls=%async_computation.3 | async-start | bytes 8519680 | tf_op jit(solution)/shard_map/all_gather | solution.py:296
  8.9 1.0 copy-start
  9.8 0.9 copy-start.1
  10.7 0.8 copy-start.2
  11.6 0.8 copy-start.3
  12.4 0.8 copy-start.4
  13.2 0.8 copy-start.5
  14.1 0.7 copy-start.6
  14.7 0.7 copy-start.7
  97.1 3.4 %copy-start.8 = (f32[2048]{0:T(1024)S(1)}, f32[2048]{0:T(1024)}, u32[]{:S(2)}) copy-start(f32[2048]{0:T(1024)} %param.22) | copy-start | bytes 24580
  101.8 53.6 %all-to-all-start = ((bf16[4,64,2048]{2,1,0:T(8,128)(2,1)}), bf16[4,64,2048]{2,1,0:T(8,128)(2,1)S(1)}, u32[]{:S(2)}, u32[]{:S(2)}) async-start(bf16[4,64,2048]{2,1,0:T(8,128)(2,1)} %broadcast_in_dim.2), calls=%async_computation | async-start | bytes 2097152 | tf_op jit(solution)/shard_map/all_to_all | solution.py:303
  161.2 19.4 %copy-start.9 = (f32[2048]{0:T(1024)S(1)}, f32[2048]{0:T(1024)}, u32[]{:S(2)}) copy-start(f32[2048]{0:T(1024)} %param.25) | copy-start | bytes 24580
Sparse Core Ops, SparseCore 0:
  9.1 53.0 all-gather.3
  65.0 84.1 all-gather.5

commit v2 on v1

v2 whole, which is shorter than its diff:
```python
import functools

import jax
import jax.numpy as jnp
from jax import lax
from jax.experimental import pallas as pl
from jax.experimental.pallas import tpu as pltpu
from jax.sharding import PartitionSpec as P

MESH = pl.DeviceIdType.MESH
NZ, NY, NX = 8, 4, 4
ALPHA = 2.0**0.5
LOG2E = 1.4426950408889634
CEXP = LOG2E * 64 ** (-0.5)
LOW = -1e30
TOK = 256
SUB = 64
NT = (((1,), (1,)), ((), ()))


def layer_norm(value, gain):
    centre = jnp.mean(value, axis=-1, keepdims=True)
    spread = jnp.mean(jnp.square(value - centre), axis=-1, keepdims=True)
    return (value - centre) * lax.rsqrt(spread + 1e-05) * gain


def layer_kernel(
    lam_ref, q1_hbm, q2_hbm, k1_hbm, k2_hbm, v_hbm, hgain_hbm, stream_hbm, ow_hbm, gain1_hbm, up_hbm, down_hbm, gain2_hbm,
    out_ref,
    q1_ref, q2_ref, k1_ref, k2_ref, v_ref, gain_ref, gain1_ref, gain2_ref,
    kvsrc, qsrc, kvbuf, qbuf, acc, mbuf, lbuf, qexp, sbuf, topbuf, osend, ssend, orecv, srecv, attown, attbuf, strbuf,
    wout, wup, wdn, hid, psend, precv, prelay,
    snd, loc, kv_rcv, q_rcv, o_rcv, s_rcv, str_rcv, att_rcv,
    upy_rcv, upz_rcv, updd_rcv, dnz_rcv, dny_rcv, dndd_rcv, ow_rcv, owdd_rcv, hid_rcv, p_rcv, pr_rcv,
):
    sp = lax.axis_index("sp")
    x = lax.axis_index("tp")
    c = lax.rem(sp, 2)
    y = lax.rem(sp // 2, NY)
    z = sp // (2 * NY)
    f = 1 - 2 * c

    def at_z(d):
        return lax.rem(z + (d + NZ), NZ)

    def at_y(d):
        return lax.rem(y + (d + NY), NY)

    def at_x(d):
        return lax.rem(x + (d + NX), NX)

    def dev(dz=0, dy=0, core=None, dx=0):
        cc = c if core is None else core
        return {"sp": (at_z(dz) * NY + at_y(dy)) * 2 + cc, "tp": at_x(dx)}

    sibling = dev(core=1 - c)
    started = []

    def send(src, dst, rcv, to):
        cp = pltpu.make_async_remote_copy(
            src_ref=src, dst_ref=dst, send_sem=snd.at[len(started)], recv_sem=rcv, device_id=to, device_id_type=MESH
        )
        cp.start()
        started.append(cp)

    def arrived(dst, rcv):
        pltpu.make_async_remote_copy(
            src_ref=dst, dst_ref=dst, send_sem=snd.at[0], recv_sem=rcv, device_id=sibling, device_id_type=MESH
        ).wait_recv()

    mine = pl.ds(pl.multiple_of(x * SUB, SUB), SUB)

    def ow_rows(d, half):
        return pl.ds(pl.multiple_of((2 * at_x(d) + half) * 128, 128), 128)

    local_pairs = [
        (q1_hbm, q1_ref), (q2_hbm, q2_ref), (k1_hbm, k1_ref), (k2_hbm, k2_ref), (v_hbm, v_ref),
        (hgain_hbm, gain_ref), (gain1_hbm, gain1_ref), (gain2_hbm, gain2_ref),
        (stream_hbm.at[mine, :], strbuf.at[x]),
        (up_hbm, wup.at[z, y, c]), (down_hbm, wdn.at[z, y, c]),
        (ow_hbm, wout.at[pl.ds(pl.multiple_of(x * 256, 256), 256), :]),
    ]
    locals_ = [pltpu.make_async_copy(a, b, loc.at[i]) for i, (a, b) in enumerate(local_pairs)]
    for cp in locals_:
        cp.start()

    barrier = pltpu.get_barrier_semaphore()
    partners = [sibling, dev(dy=2)]
    for core in (0, 1):
        partners += [dev(dz=1, core=core), dev(dz=-1, core=core), dev(dy=1, core=core), dev(dy=-1, core=core)]
        partners += [dev(dx=d, core=core) for d in (1, 2, 3)]
    for p in partners:
        pl.semaphore_signal(barrier, inc=1, device_id=p, device_id_type=MESH)

    mbuf[...] = jnp.full(mbuf.shape, LOW, jnp.float32)
    lbuf[...] = jnp.zeros(lbuf.shape, jnp.float32)

    def clear(i, carry):
        acc[i] = jnp.zeros(acc.shape[1:], jnp.float32)
        return carry

    lax.fori_loop(0, acc.shape[0], clear, 0)
    for cp in locals_[:5]:
        cp.wait()

    lane = lax.broadcasted_iota(jnp.int32, (TOK, 128), 1)
    low_half = lane < 64
    q1t = q1_ref[...].astype(jnp.float32).T.astype(jnp.bfloat16)
    q2t = q2_ref[...].astype(jnp.float32).T.astype(jnp.bfloat16)
    for h in (0, 1):
        qsrc[h, 0:64, :] = q1t[64 * h : 64 * h + 64]
        qsrc[h, 64:128, :] = q2t[64 * h : 64 * h + 64]
    vt = v_ref[...].astype(jnp.float32).T.astype(jnp.bfloat16)
    one, two = k1_ref[...].astype(jnp.float32), k2_ref[...].astype(jnp.float32)
    kvsrc[0, 0:256, :] = jnp.where(low_half, one, pltpu.roll(two, 64, 1)).astype(jnp.bfloat16)
    kvsrc[1, 0:256, :] = jnp.where(low_half, pltpu.roll(one, 64, 1), two).astype(jnp.bfloat16)
    for h in (0, 1):
        kvsrc[h, 256:384, :] = vt[128 * h : 128 * h + 128, 0:128]
        kvsrc[h, 384:512, :] = vt[128 * h : 128 * h + 128, 128:256]
    kvbuf[0, c] = kvsrc[c]
    qbuf[0, c] = qsrc[c]
    pl.semaphore_wait(barrier, len(partners))

    send(qsrc.at[1 - c], qbuf.at[0, c], q_rcv.at[0, c], sibling)
    send(kvsrc.at[1 - c], kvbuf.at[0, c], kv_rcv.at[0, c], sibling)
    for h in (0, 1):
        send(kvsrc.at[h], kvbuf.at[1, c], kv_rcv.at[1, c], dev(dz=1, core=h))
        send(kvsrc.at[h], kvbuf.at[2, c], kv_rcv.at[2, c], dev(dz=-1, core=h))
        send(qsrc.at[h], qbuf.at[1, c], q_rcv.at[1, c], dev(dy=1, core=h))
        send(qsrc.at[h], qbuf.at[2, c], q_rcv.at[2, c], dev(dy=-1, core=h))
    for dx in (1, 2, 3):
        rows = pl.ds(pl.multiple_of(at_x(dx) * SUB, SUB), SUB)
        send(stream_hbm.at[rows, :], strbuf.at[x], str_rcv.at[dx - 1], dev(dx=dx))
    half_rows = pl.ds(pl.multiple_of(c * 128, 128), 128)
    for i, d in enumerate((1, -1)):
        send(ow_hbm.at[half_rows, :], wout.at[ow_rows(0, c), :], ow_rcv.at[i], dev(dx=d))
        send(up_hbm, wup.at[z, y, c], upy_rcv.at[i], dev(dy=d))
        send(down_hbm, wdn.at[z, y, c], dnz_rcv.at[i], dev(dz=d))

    def out_weight_on():
        arrived(wout.at[ow_rows(-1, c), :], ow_rcv.at[0])
        arrived(wout.at[ow_rows(1, c), :], ow_rcv.at[1])
        blk = wout.at[ow_rows(-f, c), :]
        send(blk, blk, ow_rcv.at[2], dev(dx=f))
        for i, d in enumerate((-1, 1)):
            blk = wout.at[ow_rows(d, c), :]
            send(blk, blk, owdd_rcv.at[i], sibling)

    def out_weight_end():
        blk = wout.at[ow_rows(2, c), :]
        arrived(blk, ow_rcv.at[2])
        send(blk, blk, owdd_rcv.at[2], sibling)

    def up_y_on():
        arrived(wup.at[z, at_y(-1), c], upy_rcv.at[0])
        arrived(wup.at[z, at_y(1), c], upy_rcv.at[1])
        blk = wup.at[z, at_y(-f), c]
        send(blk, blk, upy_rcv.at[2], dev(dy=f))

    def up_y_end():
        arrived(wup.at[z, at_y(2), c], upy_rcv.at[2])
        locals_[9].wait()

    def up_z_start():
        blk = wup.at[z, :, c]
        for i, d in enumerate((1, -1)):
            send(blk, blk, upz_rcv.at[i], dev(dz=d))
        send(blk, blk, updd_rcv.at[0], sibling)

    def up_z_step(d):
        if d == 4:
            blk = wup.at[at_z(4), :, c]
            arrived(blk, upz_rcv.at[6])
            send(blk, blk, updd_rcv.at[7], sibling)
            return
        for i, s in enumerate((-1, 1)):
            blk = wup.at[at_z(s * d), :, c]
            arrived(blk, upz_rcv.at[2 * (d - 1) + i])
            if d < 3:
                send(blk, blk, upz_rcv.at[2 * d + i], dev(dz=-s))
        if d == 3:
            blk = wup.at[at_z(-3 * f), :, c]
            send(blk, blk, upz_rcv.at[6], dev(dz=f))
        for i, s in enumerate((-1, 1)):
            blk = wup.at[at_z(s * d), :, c]
            send(blk, blk, updd_rcv.at[2 * (d - 1) + 1 + i], sibling)

    def down_z_step(d):
        if d == 4:
            arrived(wdn.at[at_z(4), y, c], dnz_rcv.at[6])
            return
        for i, s in enumerate((-1, 1)):
            blk = wdn.at[at_z(s * d), y, c]
            arrived(blk, dnz_rcv.at[2 * (d - 1) + i])
            if d < 3:
                send(blk, blk, dnz_rcv.at[2 * d + i], dev(dz=-s))
        if d == 3:
            blk = wdn.at[at_z(-3 * f), y, c]
            send(blk, blk, dnz_rcv.at[6], dev(dz=f))

    def down_y_start():
        locals_[10].wait()
        blk = wdn.at[:, y, c]
        for i, d in enumerate((1, -1)):
            send(blk, blk, dny_rcv.at[i], dev(dy=d))
        send(blk, blk, dndd_rcv.at[0], sibling)

    def down_y_on():
        arrived(wdn.at[:, at_y(-1), c], dny_rcv.at[0])
        arrived(wdn.at[:, at_y(1), c], dny_rcv.at[1])
        blk = wdn.at[:, at_y(-f), c]
        send(blk, blk, dny_rcv.at[2], dev(dy=f))
        for i, d in enumerate((-1, 1)):
            blk = wdn.at[:, at_y(d), c]
            send(blk, blk, dndd_rcv.at[1 + i], sibling)

    def down_y_end():
        blk = wdn.at[:, at_y(2), c]
        arrived(blk, dny_rcv.at[2])
        send(blk, blk, dndd_rcv.at[3], sibling)

    def take_kv(slot):
        for cc in (0, 1):
            arrived(kvbuf.at[slot, cc], kv_rcv.at[slot, cc])
            step = 1 if slot % 2 else -1
            if slot <= 4:
                send(kvbuf.at[slot, cc], kvbuf.at[slot + 2, cc], kv_rcv.at[slot + 2, cc], dev(dz=step))
            elif (slot, cc) in ((5, 0), (6, 1)):
                send(kvbuf.at[slot, cc], kvbuf.at[7, cc], kv_rcv.at[7, cc], dev(dz=step))

    def take_q(slot):
        for cc in (0, 1):
            arrived(qbuf.at[slot, cc], q_rcv.at[slot, cc])
            if (slot, cc) in ((1, 0), (2, 1)):
                send(qbuf.at[slot, cc], qbuf.at[3, cc], q_rcv.at[3, cc], dev(dy=1 if slot == 1 else -1))

    def expand(qs):
        for cc in (0, 1):
            scaled = qbuf[qs, cc].astype(jnp.float32) * CEXP
            high = scaled.astype(jnp.bfloat16)
            rest = (scaled - high.astype(jnp.float32)).astype(jnp.bfloat16)
            blank = jnp.zeros((64, 256), jnp.bfloat16)
            for mp in (0, 1):
                own = slice(64 * mp, 64 * mp + 64)
                other = slice(64 - 64 * mp, 128 - 64 * mp)
                at = qs * 4 + 2 * cc + mp
                qexp[at, own, :] = high[own]
                qexp[at, other, :] = blank
                own = slice(128 + 64 * mp, 192 + 64 * mp)
                other = slice(192 - 64 * mp, 256 - 64 * mp)
                qexp[at, own, :] = rest[64 * mp : 64 * mp + 64]
                qexp[at, other, :] = blank

    def score(kvs, qs, j):
        slot = j % 4
        keys = jnp.concatenate([kvbuf[kvs, cc, 0:256, :] for cc in (0, 1)], axis=0)
        keys = jnp.concatenate([keys, keys], axis=1)
        scores = jnp.dot(keys, qexp[qs * 4 + j], preferred_element_type=jnp.float32)
        sbuf[slot] = scores
        topbuf[slot] = jnp.max(scores.reshape(64, 8, 256), axis=0)

    def absorb(kvs, qs, j):
        slot = j % 4
        at = qs * 4 + j
        vals = jnp.concatenate(
            [kvbuf[kvs, cc, 256 + 128 * i : 384 + 128 * i, :] for cc in (0, 1) for i in (0, 1)], axis=1
        )
        old = mbuf[at]
        new = jnp.maximum(old, jnp.max(topbuf[slot], axis=0, keepdims=True))
        factor = jnp.exp2(old - new)
        expo = jnp.exp2(sbuf[slot] - new)
        mbuf[at] = new
        lbuf[at] = lbuf[at] * factor + jnp.sum(expo, axis=0, keepdims=True)
        acc[at] = acc[at] * factor + jnp.dot(vals, expo.astype(jnp.bfloat16), preferred_element_type=jnp.float32)

    def process(kv_lo, kv_n, q_lo, q_n):
        last = kv_n * q_n - 1

        def place(i):
            return kv_lo + i // q_n, q_lo + lax.rem(i, q_n)

        def trip(i, carry):
            kvs, qs = place(i)
            nkvs, nqs = place(jnp.minimum(i + 1, last))
            for j in range(4):
                if j < 2:
                    score(kvs, qs, j + 2)
                else:
                    score(nkvs, nqs, j - 2)
                absorb(kvs, qs, j)
            return carry

        score(kv_lo, q_lo, 0)
        score(kv_lo, q_lo, 1)
        lax.fori_loop(0, last + 1, trip, 0)

    def finish(qs):
        for cc in (0, 1):
            for mp in (0, 1):
                at = qs * 4 + 2 * cc + mp
                osend[qs - 1, 2 * cc + mp] = (acc[at] / lbuf[at]).astype(jnp.bfloat16)
        for cc in (0, 1):
            for mp in (0, 1):
                at = qs * 4 + 2 * cc + mp
                ssend[qs - 1, 2 * cc + mp] = mbuf[at]
                ssend[qs - 1, 4 + 2 * cc + mp] = lbuf[at]
        to, land = {1: (dev(dy=-1), 1), 2: (dev(dy=1), 0), 3: (dev(dy=2), 2)}[qs]
        send(osend.at[qs - 1], orecv.at[land], o_rcv.at[land], to)
        send(ssend.at[qs - 1], srecv.at[land], s_rcv.at[land], to)

    arrived(qbuf.at[0, 1 - c], q_rcv.at[0, 1 - c])
    expand(0)
    arrived(kvbuf.at[0, 1 - c], kv_rcv.at[0, 1 - c])
    process(0, 1, 0, 1)
    take_q(1)
    take_q(2)
    expand(1)
    expand(2)
    process(0, 1, 1, 2)
    take_kv(1)
    take_kv(2)
    down_z_step(1)
    up_y_on()
    process(1, 2, 0, 3)
    take_q(3)
    expand(3)
    process(0, 3, 3, 1)
    take_kv(3)
    take_kv(4)
    down_z_step(2)
    out_weight_on()
    up_y_end()
    process(3, 2, 0, 4)
    take_kv(5)
    take_kv(6)
    down_z_step(3)
    up_z_start()
    take_kv(7)
    process(5, 3, 3, 1)
    finish(3)
    down_z_step(4)
    out_weight_end()
    process(5, 3, 1, 1)
    finish(1)
    process(5, 3, 2, 1)
    finish(2)
    down_y_start()
    up_z_step(1)
    process(5, 3, 0, 1)
    up_z_step(2)

    for j in (2, 1, 0):
        arrived(orecv.at[j], o_rcv.at[j])
        arrived(srecv.at[j], s_rcv.at[j])
    locals_[5].wait()
    lam = lam_ref[c]
    gain = gain_ref[...] * 0.8
    for cc in (0, 1):
        maps = []
        for mp in (0, 1):
            i = 2 * cc + mp
            ms = [mbuf[i]] + [srecv[j, i] for j in range(3)]
            ls = [lbuf[i]] + [srecv[j, 4 + i] for j in range(3)]
            top = functools.reduce(jnp.maximum, ms)
            ws = [jnp.exp2(m - top) for m in ms]
            total = ws[0] * ls[0]
            out = acc[i] * ws[0]
            for j in range(3):
                w = ws[j + 1] * ls[j + 1]
                total = total + w
                out = out + orecv[j, i].astype(jnp.float32) * w
            maps.append(out / total)
        mixed = maps[0] - lam * maps[1]
        inv = lax.rsqrt(jnp.mean(mixed * mixed, axis=0, keepdims=True) + 1e-5)
        attown[cc] = ((mixed * inv).T * gain).astype(jnp.bfloat16)


    head = 2 * x + c
    for dx in range(NX):
        for dc in (0, 1):
            if dx == 0 and dc == 0:
                continue
            cc = c if dc == 0 else 1 - c
            rows = pl.ds(pl.multiple_of(at_x(dx) * SUB, SUB), SUB)
            send(attown.at[cc, rows, :], attbuf.at[head], att_rcv.at[2 * dx + dc - 1], dev(dx=dx, core=cc))
    attbuf[head] = attown[c, mine, :]
    up_z_step(3)
    down_y_on()
    for i in range(3):
        arrived(wout.at[ow_rows((-1, 1, 2)[i], 1 - c), :], owdd_rcv.at[i])
    for i in (6, 7, 8, 11):
        locals_[i].wait()
    for dx in (1, 2, 3):
        arrived(strbuf.at[at_x(-dx)], str_rcv.at[dx - 1])
    for dx in range(NX):
        for dc in (0, 1):
            if dx == 0 and dc == 0:
                continue
            cc = c if dc == 0 else 1 - c
            arrived(attbuf.at[2 * at_x(-dx) + cc], att_rcv.at[2 * dx + dc - 1])
    attended = jnp.concatenate([attbuf[h] for h in range(8)], axis=1)
    rows = jnp.concatenate([strbuf[i] for i in range(NX)], axis=1).astype(jnp.float32)
    pre = ALPHA * rows + jnp.dot(attended, wout[...], preferred_element_type=jnp.float32)
    own = layer_norm(pre, gain1_ref[...]).astype(jnp.bfloat16)
    hid[x] = own
    up_z_step(4)
    for i, d in enumerate((1, -1)):
        send(hid.at[x], hid.at[x], hid_rcv.at[i], dev(dx=d))
    down_y_end()
    arrived(wup.at[z, :, 1 - c], updd_rcv.at[0])
    for d in (1, 2, 3):
        for i, s in enumerate((-1, 1)):
            arrived(wup.at[at_z(s * d), :, 1 - c], updd_rcv.at[2 * (d - 1) + 1 + i])
    arrived(wup.at[at_z(4), :, 1 - c], updd_rcv.at[7])
    arrived(wdn.at[:, y, 1 - c], dndd_rcv.at[0])
    for i, d in enumerate((-1, 1)):
        arrived(wdn.at[:, at_y(d), 1 - c], dndd_rcv.at[1 + i])
    arrived(wdn.at[:, at_y(2), 1 - c], dndd_rcv.at[3])

    def mixer(tokens):
        total = None
        for n in range(4):
            up = wup[:, :, :, :, 256 * n : 256 * n + 256].reshape(2048, 256)
            upper = jnp.dot(tokens, up, preferred_element_type=jnp.float32)
            act = jnp.square(jnp.maximum(upper, 0.0)).astype(jnp.bfloat16)
            down = wdn[:, :, :, :, 256 * n : 256 * n + 256].reshape(2048, 256)
            part = lax.dot_general(act, down, NT, preferred_element_type=jnp.float32)
            total = part if total is None else total + part
        return total

    post = mixer(own) + ALPHA * own.astype(jnp.float32)
    arrived(hid.at[at_x(-1)], hid_rcv.at[0])
    arrived(hid.at[at_x(1)], hid_rcv.at[1])
    send(hid.at[at_x(-f)], hid.at[at_x(-f)], hid_rcv.at[2], dev(dx=f))
    both = mixer(jnp.concatenate([hid[at_x(-1)], hid[at_x(1)]], axis=0)).astype(jnp.bfloat16)
    psend[0] = both[0:SUB]
    psend[1] = both[SUB:]
    send(psend.at[0], precv.at[1], p_rcv.at[1], dev(dx=-1))
    send(psend.at[1], precv.at[0], p_rcv.at[0], dev(dx=1))
    arrived(hid.at[at_x(2)], hid_rcv.at[2])
    psend[2] = mixer(hid[at_x(2)]).astype(jnp.bfloat16)
    send(psend.at[2], prelay, pr_rcv.at[0], dev(dx=f))
    arrived(prelay, pr_rcv.at[0])
    send(prelay, precv.at[2], p_rcv.at[2], dev(dx=f))
    for i in range(3):
        arrived(precv.at[i], p_rcv.at[i])
        post = post + precv[i].astype(jnp.float32)
    out_ref[...] = layer_norm(post, gain2_ref[...]).astype(jnp.bfloat16)
    for cp in started:
        cp.wait_send()


def local(
    query_one, query_two, key_one, key_two, values, mix_lambda, head_gain, stream, out_weight, first_gain,
    up_weight, down_weight, second_gain,
):
    bf, f32 = jnp.bfloat16, jnp.float32
    hbm = pl.BlockSpec(memory_space=pltpu.HBM)
    dma = pltpu.SemaphoreType.DMA
    return pl.pallas_call(
        layer_kernel,
        out_shape=jax.ShapeDtypeStruct((SUB, 2048), bf),
        in_specs=[pl.BlockSpec(memory_space=pltpu.SMEM)] + [hbm] * 12,
        out_specs=pl.BlockSpec(memory_space=pltpu.VMEM),
        scratch_shapes=[
            pltpu.VMEM((256, 128), bf),
            pltpu.VMEM((256, 128), bf),
            pltpu.VMEM((256, 128), bf),
            pltpu.VMEM((256, 128), bf),
            pltpu.VMEM((256, 256), bf),
            pltpu.VMEM((1, 128), f32),
            pltpu.VMEM((1, 2048), f32),
            pltpu.VMEM((1, 2048), f32),
            pltpu.VMEM((2, 512, 128), bf),
            pltpu.VMEM((2, 128, 256), bf),
            pltpu.VMEM((8, 2, 512, 128), bf),
            pltpu.VMEM((4, 2, 128, 256), bf),
            pltpu.VMEM((16, 128, 256), f32),
            pltpu.VMEM((16, 1, 256), f32),
            pltpu.VMEM((16, 1, 256), f32),
            pltpu.VMEM((16, 256, 256), bf),
            pltpu.VMEM((4, 512, 256), f32),
            pltpu.VMEM((4, 8, 256), f32),
            pltpu.VMEM((3, 4, 128, 256), bf),
            pltpu.VMEM((3, 8, 1, 256), f32),
            pltpu.VMEM((3, 4, 128, 256), bf),
            pltpu.VMEM((3, 8, 1, 256), f32),
            pltpu.VMEM((2, 256, 128), bf),
            pltpu.VMEM((8, SUB, 128), bf),
            pltpu.VMEM((NX, SUB, 512), bf),
            pltpu.VMEM((1024, 2048), bf),
            pltpu.VMEM((NZ, NY, 2, 32, 1024), bf),
            pltpu.VMEM((NZ, NY, 2, 32, 1024), bf),
            pltpu.VMEM((NX, SUB, 2048), bf),
            pltpu.VMEM((3, SUB, 2048), bf),
            pltpu.VMEM((3, SUB, 2048), bf),
            pltpu.VMEM((SUB, 2048), bf),
            dma((96,)),
            dma((12,)),
            dma((8, 2)),
            dma((4, 2)),
            dma((3,)),
            dma((3,)),
            dma((3,)),
            dma((7,)),
            dma((3,)),
            dma((7,)),
            dma((8,)),
            dma((7,)),
            dma((3,)),
            dma((4,)),
            dma((3,)),
            dma((3,)),
            dma((3,)),
            dma((3,)),
            dma((1,)),
        ],
        compiler_params=pltpu.CompilerParams(
            collective_id=0, has_side_effects=True, vmem_limit_bytes=56 * 1024 * 1024
        ),
        cost_estimate=pl.CostEstimate(flops=20_000_000_000, bytes_accessed=4_000_000, transcendentals=17_000_000),
        name="layer",
    )(
        mix_lambda, query_one, query_two, key_one, key_two, values, head_gain.reshape(1, 128), stream, out_weight,
        first_gain.reshape(1, 2048), up_weight, down_weight.T, second_gain.reshape(1, 2048),
    )


def solution(mesh):
    in_specs = (
        P("sp", "tp"), P("sp", "tp"), P("sp", "tp"), P("sp", "tp"), P("sp", "tp"), P("tp"), P(), P("sp", "tp"),
        P("tp", None), P(), P("sp", "tp"), P("tp", "sp"), P(),
    )
    return jax.shard_map(
        local, mesh=mesh, in_specs=in_specs, out_specs=P(("sp", "tp"), None), check_vma=False
    )
```

time: 190 us -> 101 us (0.53)
  waiting for transfers between devices: 42.9 us -> 0 us
  blocking collectives: 18.7 us -> 0 us
  Pallas kernels: 81.7 us -> 98 us
  between operations: 13.5 us -> 0.01 us
  local copies, waits for them, and re-layouts: 13.9 us -> 1.67 us
  matrix products: 8.95 us -> 0 us
  starting transfers between devices: 5.32 us -> 0 us
  other arithmetic: 3.64 us -> 0 us
    all_gather x2 -> x0, waiting for transfers between devices: 42.1 us -> none  [the longest x1 42.1 us: local(): weights = lax.all_gather(both, 'sp', axis=0, tiled=False)]
    all_to_all x1 -> x0, blocking collectives: 18.7 us -> none  [local(): parts = lax.all_to_all(part.reshape(NX, SUB, 2048), 'tp', 0, 0, tiled=True)]
    pallas_call x1, Pallas kernels: 81.7 us -> 98 us  [local(): pl.pallas_call(layer_kernel, out_shape=jax.ShapeDtypeStruct((SUB, 2048),...]
    dot_general x2 -> x0, matrix products: 8.95 us -> none  [the longest x1 5.81 us: local(): lax.dot_general(act, down_t, NT, preferred_element_type=f32).astype(bf)]
    slice x1 -> x0, local copies, waits for them, and re-layouts: 6.24 us -> none  [local(): up_full = weights[:, 0:32, :].reshape(2048, 1024)]
    all_to_all x1 -> x0, starting transfers between devices: 5.27 us -> none  [local(): lax.all_to_all(jnp.broadcast_to(own, (NX, *own.shape)), 'tp', 0, 0, tiled...]
    unnamed x20 -> x1, local copies, waits for them, and re-layouts: 6.53 us -> 1.67 us
  transfers between devices with their start and end apart: 3 -> 0, of which waited for: 1 -> 0; matrix products, arithmetic and copies ran while one was open for 7% -> 0% of each run, Pallas kernels for 43% -> 0%
where the time goes in v2:
time: 101 us; the launch traced here: 99.7 us
  Pallas kernels  98 us (97%)
  local copies, waits for them, and re-layouts  1.67 us (2%)
    pallas_call x1, Pallas kernels, local(): pl.pallas_call(layer_kernel, out_shape=jax.ShapeDtypeStruct((SUB, 2048),...  98 us

profile of v2, /device:TPU:2, one launch (start us, length us, event | category | flops | bytes accessed | tf_op | source)
XLA Modules:
  0.0 99.7 jit_solution(3736041953175022308)
XLA Ops:
  0.0 98.0 %layer.1 = bf16[64,2048]{1,0:T(8,128)(2,1)} custom-call(f32[2]{0:T(128)} %lam_ref.1, bf16[256,128]{1,0:T(8,128)(2,1)} %q1_hbm.1, bf16[256,128]{1,0:T(8,128)(2,1)} %q2_hbm.1, bf16[256,128]{1,0:T(8,128)(2,1)} %k1_hbm.1, bf16[256,128]{1,0:T(8,128)(2,1)} %k2_hbm.1, bf16[256,256]{1,0:T(8,128)(2,1)} %v_hbm.1, f32[1,128]{1,0:T(1,128)} %bitcast.7, ...), custom_call_target="tpu_custom_call" | custom-call | flops 20000000000 | bytes 4000000 | tf_op jit(solution)/shard_map/layer/pallas_call | solution.py:460
  98.0 1.7 %copy.15 = bf16[64,2048]{1,0:T(8,128)(2,1)} copy(bf16[64,2048]{1,0:T(8,128)(2,1)} %layer.1) | data formatting | bytes 524288

commit v3 on v2

--- a/solution.py
+++ b/solution.py
@@ -29,9 +29,9 @@
     out_ref,
     q1_ref, q2_ref, k1_ref, k2_ref, v_ref, gain_ref, gain1_ref, gain2_ref,
     kvsrc, qsrc, kvbuf, qbuf, acc, mbuf, lbuf, qexp, sbuf, topbuf, osend, ssend, orecv, srecv, attown, attbuf, strbuf,
-    wout, wup, wdn, hid, psend, precv, prelay,
+    wout, wup, wdn, hid, psend, precv, pown, prelay, orelay, srelay, wdnt,
     snd, loc, kv_rcv, q_rcv, o_rcv, s_rcv, str_rcv, att_rcv,
-    upy_rcv, upz_rcv, updd_rcv, dnz_rcv, dny_rcv, dndd_rcv, ow_rcv, owdd_rcv, hid_rcv, p_rcv, pr_rcv,
+    upy_rcv, upz_rcv, updd_rcv, dnz_rcv, dny_rcv, dndd_rcv, ow_rcv, owdd_rcv, hid_rcv, p_rcv, pr_rcv, or_rcv,
 ):
     sp = lax.axis_index("sp")
     x = lax.axis_index("tp")
@@ -123,19 +123,20 @@
 
     send(qsrc.at[1 - c], qbuf.at[0, c], q_rcv.at[0, c], sibling)
     send(kvsrc.at[1 - c], kvbuf.at[0, c], kv_rcv.at[0, c], sibling)
+    for i, d in enumerate((1, -1)):
+        send(down_hbm, wdn.at[z, y, c], dnz_rcv.at[i], dev(dz=d))
     for h in (0, 1):
+        send(qsrc.at[h], qbuf.at[1, c], q_rcv.at[1, c], dev(dy=1, core=h))
+        send(qsrc.at[h], qbuf.at[2, c], q_rcv.at[2, c], dev(dy=-1, core=h))
         send(kvsrc.at[h], kvbuf.at[1, c], kv_rcv.at[1, c], dev(dz=1, core=h))
         send(kvsrc.at[h], kvbuf.at[2, c], kv_rcv.at[2, c], dev(dz=-1, core=h))
-        send(qsrc.at[h], qbuf.at[1, c], q_rcv.at[1, c], dev(dy=1, core=h))
-        send(qsrc.at[h], qbuf.at[2, c], q_rcv.at[2, c], dev(dy=-1, core=h))
     for dx in (1, 2, 3):
         rows = pl.ds(pl.multiple_of(at_x(dx) * SUB, SUB), SUB)
         send(stream_hbm.at[rows, :], strbuf.at[x], str_rcv.at[dx - 1], dev(dx=dx))
     half_rows = pl.ds(pl.multiple_of(c * 128, 128), 128)
     for i, d in enumerate((1, -1)):
+        send(up_hbm, wup.at[z, y, c], upy_rcv.at[i], dev(dy=d))
         send(ow_hbm.at[half_rows, :], wout.at[ow_rows(0, c), :], ow_rcv.at[i], dev(dx=d))
-        send(up_hbm, wup.at[z, y, c], upy_rcv.at[i], dev(dy=d))
-        send(down_hbm, wdn.at[z, y, c], dnz_rcv.at[i], dev(dz=d))
 
     def out_weight_on():
         arrived(wout.at[ow_rows(-1, c), :], ow_rcv.at[0])
@@ -273,7 +274,7 @@
         lbuf[at] = lbuf[at] * factor + jnp.sum(expo, axis=0, keepdims=True)
         acc[at] = acc[at] * factor + jnp.dot(vals, expo.astype(jnp.bfloat16), preferred_element_type=jnp.float32)
 
-    def process(kv_lo, kv_n, q_lo, q_n):
+    def process(kv_lo, kv_n, q_lo, q_n, ready=False, then=None):
         last = kv_n * q_n - 1
 
         def place(i):
@@ -282,6 +283,8 @@
         def trip(i, carry):
             kvs, qs = place(i)
             nkvs, nqs = place(jnp.minimum(i + 1, last))
+            if then is not None:
+                nkvs, nqs = jnp.where(i == last, then[0], nkvs), jnp.where(i == last, then[1], nqs)
             for j in range(4):
                 if j < 2:
                     score(kvs, qs, j + 2)
@@ -290,66 +293,93 @@
                 absorb(kvs, qs, j)
             return carry
 
-        score(kv_lo, q_lo, 0)
-        score(kv_lo, q_lo, 1)
+        if not ready:
+            score(kv_lo, q_lo, 0)
+            score(kv_lo, q_lo, 1)
         lax.fori_loop(0, last + 1, trip, 0)
 
-    def finish(qs):
-        for cc in (0, 1):
-            for mp in (0, 1):
-                at = qs * 4 + 2 * cc + mp
-                osend[qs - 1, 2 * cc + mp] = (acc[at] / lbuf[at]).astype(jnp.bfloat16)
-        for cc in (0, 1):
-            for mp in (0, 1):
-                at = qs * 4 + 2 * cc + mp
-                ssend[qs - 1, 2 * cc + mp] = mbuf[at]
-                ssend[qs - 1, 4 + 2 * cc + mp] = lbuf[at]
-        to, land = {1: (dev(dy=-1), 1), 2: (dev(dy=1), 0), 3: (dev(dy=2), 2)}[qs]
-        send(osend.at[qs - 1], orecv.at[land], o_rcv.at[land], to)
-        send(ssend.at[qs - 1], srecv.at[land], s_rcv.at[land], to)
+    q_direct, q_merged = (3 - f) // 2, (3 + f) // 2
+
+    def finish(qs, place):
+        for i in range(4):
+            osend[place, i] = (acc[qs * 4 + i] / lbuf[qs * 4 + i]).astype(jnp.bfloat16)
+        for i in range(4):
+            ssend[place, i] = mbuf[qs * 4 + i]
+            ssend[place, 4 + i] = lbuf[qs * 4 + i]
+
+    def opposite_out():
+        finish(3, 0)
+        send(osend.at[0], orelay, or_rcv.at[0], dev(dy=f))
+        send(ssend.at[0], srelay, or_rcv.at[1], dev(dy=f))
+
+    def direct_out():
+        finish(q_direct, 1)
+        send(osend.at[1], orecv.at[0], o_rcv.at[0], dev(dy=-f))
+        send(ssend.at[1], srecv.at[0], s_rcv.at[0], dev(dy=-f))
+
+    def merged_out():
+        arrived(orelay, or_rcv.at[0])
+        arrived(srelay, or_rcv.at[1])
+        for i in range(4):
+            m, l = mbuf[q_merged * 4 + i], lbuf[q_merged * 4 + i]
+            top = jnp.maximum(m, srelay[i])
+            w, v = jnp.exp2(m - top), jnp.exp2(srelay[i] - top) * srelay[4 + i]
+            total = l * w + v
+            osend[2, i] = (
+                acc[q_merged * 4 + i] * (w / total) + orelay[i].astype(jnp.float32) * (v / total)
+            ).astype(jnp.bfloat16)
+            ssend[2, i] = top
+            ssend[2, 4 + i] = total
+        send(osend.at[2], orecv.at[1], o_rcv.at[1], dev(dy=f))
+        send(ssend.at[2], srecv.at[1], s_rcv.at[1], dev(dy=f))
 
     arrived(qbuf.at[0, 1 - c], q_rcv.at[0, 1 - c])
     expand(0)
     arrived(kvbuf.at[0, 1 - c], kv_rcv.at[0, 1 - c])
     process(0, 1, 0, 1)
+    down_z_step(1)
     take_q(1)
     take_q(2)
     expand(1)
     expand(2)
     process(0, 1, 1, 2)
+    down_z_step(2)
     take_kv(1)
     take_kv(2)
-    down_z_step(1)
     up_y_on()
-    process(1, 2, 0, 3)
+    process(1, 1, 0, 3)
     take_q(3)
     expand(3)
-    process(0, 3, 3, 1)
+    down_z_step(3)
+    process(0, 2, 3, 1)
     take_kv(3)
     take_kv(4)
-    down_z_step(2)
+    down_z_step(4)
+    down_y_start()
     out_weight_on()
     up_y_end()
-    process(3, 2, 0, 4)
+    process(2, 1, 0, 4, then=(3, 0))
+    up_z_start()
+    process(3, 1, 0, 4, ready=True)
     take_kv(5)
     take_kv(6)
-    down_z_step(3)
-    up_z_start()
+    process(4, 1, 0, 4, then=(5, 3))
+    process(5, 2, 3, 1, ready=True, then=(5, q_direct))
+    process(5, 2, q_direct, 1, ready=True)
+    out_weight_end()
     take_kv(7)
-    process(5, 3, 3, 1)
-    finish(3)
-    down_z_step(4)
-    out_weight_end()
-    process(5, 3, 1, 1)
-    finish(1)
-    process(5, 3, 2, 1)
-    finish(2)
-    down_y_start()
+    process(7, 1, 3, 1, then=(7, q_direct))
+    opposite_out()
+    process(7, 1, q_direct, 1, ready=True, then=(5, q_merged))
+    direct_out()
     up_z_step(1)
-    process(5, 3, 0, 1)
+    process(5, 3, q_merged, 1, ready=True, then=(5, 0))
+    process(5, 3, 0, 1, ready=True)
+    merged_out()
+    down_y_on()
     up_z_step(2)
 
-    for j in (2, 1, 0):
+    for j in (0, 1):
         arrived(orecv.at[j], o_rcv.at[j])
         arrived(srecv.at[j], s_rcv.at[j])
     locals_[5].wait()
@@ -359,13 +389,13 @@
         maps = []
         for mp in (0, 1):
             i = 2 * cc + mp
-            ms = [mbuf[i]] + [srecv[j, i] for j in range(3)]
-            ls = [lbuf[i]] + [srecv[j, 4 + i] for j in range(3)]
+            ms = [mbuf[i]] + [srecv[j, i] for j in range(2)]
+            ls = [lbuf[i]] + [srecv[j, 4 + i] for j in range(2)]
             top = functools.reduce(jnp.maximum, ms)
             ws = [jnp.exp2(m - top) for m in ms]
             total = ws[0] * ls[0]
             out = acc[i] * ws[0]
-            for j in range(3):
+            for j in range(2):
                 w = ws[j + 1] * ls[j + 1]
                 total = total + w
                 out = out + orecv[j, i].astype(jnp.float32) * w
@@ -385,7 +415,6 @@
             send(attown.at[cc, rows, :], attbuf.at[head], att_rcv.at[2 * dx + dc - 1], dev(dx=dx, core=cc))
     attbuf[head] = attown[c, mine, :]
     up_z_step(3)
-    down_y_on()
     for i in range(3):
         arrived(wout.at[ow_rows((-1, 1, 2)[i], 1 - c), :], owdd_rcv.at[i])
     for i in (6, 7, 8, 11):
@@ -403,19 +432,23 @@
     pre = ALPHA * rows + jnp.dot(attended, wout[...], preferred_element_type=jnp.float32)
     own = layer_norm(pre, gain1_ref[...]).astype(jnp.bfloat16)
     hid[x] = own
+    down_y_end()
+    halves = [pl.ds(i * (SUB // 2), SUB // 2) for i in (0, 1)]
+    for n, half in enumerate(halves):
+        for i, d in enumerate((f, -f)):
+            send(hid.at[x, half, :], hid.at[x, half, :], hid_rcv.at[2 * i + n], dev(dx=d))
     up_z_step(4)
-    for i, d in enumerate((1, -1)):
-        send(hid.at[x], hid.at[x], hid_rcv.at[i], dev(dx=d))
-    down_y_end()
+    arrived(wdn.at[:, y, 1 - c], dndd_rcv.at[0])
+    for i, d in enumerate((-1, 1)):
+        arrived(wdn.at[:, at_y(d), 1 - c], dndd_rcv.at[1 + i])
+    arrived(wdn.at[:, at_y(2), 1 - c], dndd_rcv.at[3])
+    for i in range(NZ):
+        wdnt[:, 256 * i : 256 * i + 256] = wdn[i].reshape(256, 1024).T
     arrived(wup.at[z, :, 1 - c], updd_rcv.at[0])
     for d in (1, 2, 3):
         for i, s in enumerate((-1, 1)):
             arrived(wup.at[at_z(s * d), :, 1 - c], updd_rcv.at[2 * (d - 1) + 1 + i])
     arrived(wup.at[at_z(4), :, 1 - c], updd_rcv.at[7])
-    arrived(wdn.at[:, y, 1 - c], dndd_rcv.at[0])
-    for i, d in enumerate((-1, 1)):
-        arrived(wdn.at[:, at_y(d), 1 - c], dndd_rcv.at[1 + i])
-    arrived(wdn.at[:, at_y(2), 1 - c], dndd_rcv.at[3])
 
     def mixer(tokens):
         total = None
@@ -423,27 +456,35 @@
             up = wup[:, :, :, :, 256 * n : 256 * n + 256].reshape(2048, 256)
             upper = jnp.dot(tokens, up, preferred_element_type=jnp.float32)
             act = jnp.square(jnp.maximum(upper, 0.0)).astype(jnp.bfloat16)
-            down = wdn[:, :, :, :, 256 * n : 256 * n + 256].reshape(2048, 256)
-            part = lax.dot_general(act, down, NT, preferred_element_type=jnp.float32)
+            part = jnp.dot(act, wdnt[256 * n : 256 * n + 256, :], preferred_element_type=jnp.float32)
             total = part if total is None else total + part
         return total
 
     post = mixer(own) + ALPHA * own.astype(jnp.float32)
-    arrived(hid.at[at_x(-1)], hid_rcv.at[0])
-    arrived(hid.at[at_x(1)], hid_rcv.at[1])
-    send(hid.at[at_x(-f)], hid.at[at_x(-f)], hid_rcv.at[2], dev(dx=f))
-    both = mixer(jnp.concatenate([hid[at_x(-1)], hid[at_x(1)]], axis=0)).astype(jnp.bfloat16)
-    psend[0] = both[0:SUB]
-    psend[1] = both[SUB:]
-    send(psend.at[0], precv.at[1], p_rcv.at[1], dev(dx=-1))
-    send(psend.at[1], precv.at[0], p_rcv.at[0], dev(dx=1))
-    arrived(hid.at[at_x(2)], hid_rcv.at[2])
-    psend[2] = mixer(hid[at_x(2)]).astype(jnp.bfloat16)
-    send(psend.at[2], prelay, pr_rcv.at[0], dev(dx=f))
-    arrived(prelay, pr_rcv.at[0])
-    send(prelay, precv.at[2], p_rcv.at[2], dev(dx=f))
-    for i in range(3):
-        arrived(precv.at[i], p_rcv.at[i])
+    for n, half in enumerate(halves):
+        blk = hid.at[at_x(-f), half, :]
+        arrived(blk, hid_rcv.at[n])
+        send(blk, blk, hid_rcv.at[4 + n], dev(dx=f))
+    for n, half in enumerate(halves):
+        arrived(hid.at[at_x(f), half, :], hid_rcv.at[2 + n])
+    both = mixer(jnp.concatenate([hid[at_x(-f)], hid[at_x(f)]], axis=0))
+    psend[0] = both[0:SUB].astype(jnp.bfloat16)
+    pown[...] = both[SUB:]
+    send(psend.at[0], precv.at[0], p_rcv.at[0], dev(dx=-f))
+    for n, half in enumerate(halves):
+        arrived(hid.at[at_x(2), half, :], hid_rcv.at[4 + n])
+    psend[1] = mixer(hid[at_x(2)]).astype(jnp.bfloat16)
+    quarters = [pl.ds(i * (SUB // 4), SUB // 4) for i in range(4)]
+    for i, part in enumerate(quarters):
+        send(psend.at[1, part, :], prelay.at[i], pr_rcv.at[i], dev(dx=f))
+    for i, part in enumerate(quarters):
+        arrived(prelay.at[i], pr_rcv.at[i])
+        psend[2, part, :] = (pown[part, :] + prelay[i].astype(jnp.float32)).astype(jnp.bfloat16)
+        send(psend.at[2, part, :], precv.at[1, part, :], p_rcv.at[1 + i], dev(dx=f))
+    arrived(precv.at[0], p_rcv.at[0])
+    for i, part in enumerate(quarters):
+        arrived(precv.at[1, part, :], p_rcv.at[1 + i])
+    for i in range(2):
         post = post + precv[i].astype(jnp.float32)
     out_ref[...] = layer_norm(post, gain2_ref[...]).astype(jnp.bfloat16)
     for cp in started:
@@ -483,8 +524,8 @@
             pltpu.VMEM((4, 8, 256), f32),
             pltpu.VMEM((3, 4, 128, 256), bf),
             pltpu.VMEM((3, 8, 1, 256), f32),
-            pltpu.VMEM((3, 4, 128, 256), bf),
-            pltpu.VMEM((3, 8, 1, 256), f32),
+            pltpu.VMEM((2, 4, 128, 256), bf),
+            pltpu.VMEM((2, 8, 1, 256), f32),
             pltpu.VMEM((2, 256, 128), bf),
             pltpu.VMEM((8, SUB, 128), bf),
             pltpu.VMEM((NX, SUB, 512), bf),
@@ -493,9 +534,13 @@
             pltpu.VMEM((NZ, NY, 2, 32, 1024), bf),
             pltpu.VMEM((NX, SUB, 2048), bf),
             pltpu.VMEM((3, SUB, 2048), bf),
-            pltpu.VMEM((3, SUB, 2048), bf),
-            pltpu.VMEM((SUB, 2048), bf),
-            dma((96,)),
+            pltpu.VMEM((2, SUB, 2048), bf),
+            pltpu.VMEM((SUB, 2048), f32),
+            pltpu.VMEM((4, SUB // 4, 2048), bf),
+            pltpu.VMEM((4, 128, 256), bf),
+            pltpu.VMEM((8, 1, 256), f32),
+            pltpu.VMEM((1024, 2048), bf),
+            dma((128,)),
             dma((12,)),
             dma((8, 2)),
             dma((4, 2)),
@@ -511,9 +556,10 @@
             dma((4,)),
             dma((3,)),
             dma((3,)),
-            dma((3,)),
-            dma((3,)),
-            dma((1,)),
+            dma((6,)),
+            dma((6,)),
+            dma((4,)),
+            dma((2,)),
         ],
         compiler_params=pltpu.CompilerParams(
             collective_id=0, has_side_effects=True, vmem_limit_bytes=56 * 1024 * 1024

time: 101 us -> 91 us (0.901)
  Pallas kernels: 98 us -> 88.8 us
    pallas_call x1, Pallas kernels: 98 us -> 88.8 us  [local(): pl.pallas_call(layer_kernel, out_shape=jax.ShapeDtypeStruct((SUB, 2048),...]
where the time goes in v3:
time: 91 us; the launch traced here: 90.4 us
  Pallas kernels  88.8 us (98%)
  local copies, waits for them, and re-layouts  1.67 us (2%)
    pallas_call x1, Pallas kernels, local(): pl.pallas_call(layer_kernel, out_shape=jax.ShapeDtypeStruct((SUB, 2048),...  88.8 us

profile of v3, /device:TPU:2, one launch (start us, length us, event | category | flops | bytes accessed | tf_op | source)
XLA Modules:
  0.0 90.4 jit_solution(7410829808150024337)
XLA Ops:
  0.0 88.8 %layer.1 = bf16[64,2048]{1,0:T(8,128)(2,1)} custom-call(f32[2]{0:T(128)} %lam_ref.1, bf16[256,128]{1,0:T(8,128)(2,1)} %q1_hbm.1, bf16[256,128]{1,0:T(8,128)(2,1)} %q2_hbm.1, bf16[256,128]{1,0:T(8,128)(2,1)} %k1_hbm.1, bf16[256,128]{1,0:T(8,128)(2,1)} %k2_hbm.1, bf16[256,256]{1,0:T(8,128)(2,1)} %v_hbm.1, f32[1,128]{1,0:T(1,128)} %bitcast.7, ...), custom_call_target="tpu_custom_call" | custom-call | flops 20000000000 | bytes 4000000 | tf_op jit(solution)/shard_map/layer/pallas_call | solution.py:501
  88.8 1.7 %copy.15 = bf16[64,2048]{1,0:T(8,128)(2,1)} copy(bf16[64,2048]{1,0:T(8,128)(2,1)} %layer.1) | data formatting | bytes 524288

commit v4 on v3

--- a/solution.py
+++ b/solution.py
@@ -119,12 +119,14 @@
         kvsrc[h, 384:512, :] = vt[128 * h : 128 * h + 128, 128:256]
     kvbuf[0, c] = kvsrc[c]
     qbuf[0, c] = qsrc[c]
+    for i in (9, 10, 11):
+        locals_[i].wait()
     pl.semaphore_wait(barrier, len(partners))
 
     send(qsrc.at[1 - c], qbuf.at[0, c], q_rcv.at[0, c], sibling)
     send(kvsrc.at[1 - c], kvbuf.at[0, c], kv_rcv.at[0, c], sibling)
     for i, d in enumerate((1, -1)):
-        send(down_hbm, wdn.at[z, y, c], dnz_rcv.at[i], dev(dz=d))
+        send(wdn.at[z, y, c], wdn.at[z, y, c], dnz_rcv.at[i], dev(dz=d))
     for h in (0, 1):
         send(qsrc.at[h], qbuf.at[1, c], q_rcv.at[1, c], dev(dy=1, core=h))
         send(qsrc.at[h], qbuf.at[2, c], q_rcv.at[2, c], dev(dy=-1, core=h))
@@ -133,10 +135,8 @@
     for dx in (1, 2, 3):
         rows = pl.ds(pl.multiple_of(at_x(dx) * SUB, SUB), SUB)
         send(stream_hbm.at[rows, :], strbuf.at[x], str_rcv.at[dx - 1], dev(dx=dx))
-    half_rows = pl.ds(pl.multiple_of(c * 128, 128), 128)
     for i, d in enumerate((1, -1)):
-        send(up_hbm, wup.at[z, y, c], upy_rcv.at[i], dev(dy=d))
-        send(ow_hbm.at[half_rows, :], wout.at[ow_rows(0, c), :], ow_rcv.at[i], dev(dx=d))
+        send(wout.at[ow_rows(0, c), :], wout.at[ow_rows(0, c), :], ow_rcv.at[i], dev(dx=d))
 
     def out_weight_on():
         arrived(wout.at[ow_rows(-1, c), :], ow_rcv.at[0])
@@ -152,6 +152,10 @@
         arrived(blk, ow_rcv.at[2])
         send(blk, blk, owdd_rcv.at[2], sibling)
 
+    def up_y_start():
+        for i, d in enumerate((1, -1)):
+            send(wup.at[z, y, c], wup.at[z, y, c], upy_rcv.at[i], dev(dy=d))
+
     def up_y_on():
         arrived(wup.at[z, at_y(-1), c], upy_rcv.at[0])
         arrived(wup.at[z, at_y(1), c], upy_rcv.at[1])
@@ -160,7 +164,6 @@
 
     def up_y_end():
         arrived(wup.at[z, at_y(2), c], upy_rcv.at[2])
-        locals_[9].wait()
 
     def up_z_start():
         blk = wup.at[z, :, c]
@@ -199,26 +202,33 @@
             blk = wdn.at[at_z(-3 * f), y, c]
             send(blk, blk, dnz_rcv.at[6], dev(dz=f))
 
-    def down_y_start():
-        locals_[10].wait()
-        blk = wdn.at[:, y, c]
-        for i, d in enumerate((1, -1)):
-            send(blk, blk, dny_rcv.at[i], dev(dy=d))
-        send(blk, blk, dndd_rcv.at[0], sibling)
-
-    def down_y_on():
-        arrived(wdn.at[:, at_y(-1), c], dny_rcv.at[0])
-        arrived(wdn.at[:, at_y(1), c], dny_rcv.at[1])
-        blk = wdn.at[:, at_y(-f), c]
-        send(blk, blk, dny_rcv.at[2], dev(dy=f))
-        for i, d in enumerate((-1, 1)):
-            blk = wdn.at[:, at_y(d), c]
-            send(blk, blk, dndd_rcv.at[1 + i], sibling)
-
-    def down_y_end():
-        blk = wdn.at[:, at_y(2), c]
-        arrived(blk, dny_rcv.at[2])
-        send(blk, blk, dndd_rcv.at[3], sibling)
+    def down_zs(g):
+        return {0: ((0, 0),), 1: ((-1, 3), (1, 6)), 2: ((-2, 9), (2, 12)), 3: ((-3, 15), (3, 18)), 4: ((4, 21),)}[g]
+
+    def down_y_start(g):
+        for dz, k in down_zs(g):
+            blk = wdn.at[at_z(dz), y, c]
+            for i, d in enumerate((1, -1)):
+                send(blk, blk, dny_rcv.at[k + i], dev(dy=d))
+
+    def down_y_on(g):
+        for dz, k in down_zs(g):
+            for i, d in enumerate((-1, 1)):
+                arrived(wdn.at[at_z(dz), at_y(d), c], dny_rcv.at[k + i])
+            blk = wdn.at[at_z(dz), at_y(-f), c]
+            send(blk, blk, dny_rcv.at[k + 2], dev(dy=f))
+
+    def down_y_end(g):
+        for dz, k in down_zs(g):
+            arrived(wdn.at[at_z(dz), at_y(2), c], dny_rcv.at[k + 2])
+
+    def down_over(i):
+        blk = wdn.at[:, at_y((0, -1, 1, 2)[i]), c]
+        send(blk, blk, dndd_rcv.at[i], sibling)
+
+    def down_here():
+        for i, d in enumerate((0, -1, 1, 2)):
+            arrived(wdn.at[:, at_y(d), 1 - c], dndd_rcv.at[i])
 
     def take_kv(slot):
         for cc in (0, 1):
@@ -340,44 +350,53 @@
     down_z_step(1)
     take_q(1)
     take_q(2)
+    up_y_start()
+    down_y_start(0)
+    down_y_start(1)
     expand(1)
     expand(2)
     process(0, 1, 1, 2)
-    down_z_step(2)
     take_kv(1)
     take_kv(2)
-    up_y_on()
     process(1, 1, 0, 3)
     take_q(3)
     expand(3)
-    down_z_step(3)
+    down_z_step(2)
+    down_y_start(2)
     process(0, 2, 3, 1)
     take_kv(3)
     take_kv(4)
-    down_z_step(4)
-    down_y_start()
-    out_weight_on()
+    up_y_on()
+    down_y_on(0)
+    process(2, 1, 0, 4, then=(3, 0))
+    down_z_step(3)
+    down_y_start(3)
+    down_y_on(1)
     up_y_end()
-    process(2, 1, 0, 4, then=(3, 0))
-    up_z_start()
     process(3, 1, 0, 4, ready=True)
     take_kv(5)
     take_kv(6)
+    up_z_start()
+    down_y_on(2)
+    out_weight_on()
     process(4, 1, 0, 4, then=(5, 3))
     process(5, 2, 3, 1, ready=True, then=(5, q_direct))
+    down_z_step(4)
+    down_y_start(4)
+    down_y_on(3)
+    down_over(0)
     process(5, 2, q_direct, 1, ready=True)
-    out_weight_end()
     take_kv(7)
     process(7, 1, 3, 1, then=(7, q_direct))
     opposite_out()
     process(7, 1, q_direct, 1, ready=True, then=(5, q_merged))
+    process(5, 3, q_merged, 1, ready=True, then=(5, 0))
     direct_out()
+    out_weight_end()
+    process(5, 3, 0, 1, ready=True)
     up_z_step(1)
-    process(5, 3, q_merged, 1, ready=True, then=(5, 0))
-    process(5, 3, 0, 1, ready=True)
     merged_out()
-    down_y_on()
-    up_z_step(2)
+    down_y_on(4)
 
     for j in (0, 1):
         arrived(orecv.at[j], o_rcv.at[j])
@@ -414,10 +433,12 @@
             rows = pl.ds(pl.multiple_of(at_x(dx) * SUB, SUB), SUB)
             send(attown.at[cc, rows, :], attbuf.at[head], att_rcv.at[2 * dx + dc - 1], dev(dx=dx, core=cc))
     attbuf[head] = attown[c, mine, :]
-    up_z_step(3)
+    up_z_step(2)
+    down_over(1)
+    down_over(2)
     for i in range(3):
         arrived(wout.at[ow_rows((-1, 1, 2)[i], 1 - c), :], owdd_rcv.at[i])
-    for i in (6, 7, 8, 11):
+    for i in (6, 7, 8):
         locals_[i].wait()
     for dx in (1, 2, 3):
         arrived(strbuf.at[at_x(-dx)], str_rcv.at[dx - 1])
@@ -432,18 +453,23 @@
     pre = ALPHA * rows + jnp.dot(attended, wout[...], preferred_element_type=jnp.float32)
     own = layer_norm(pre, gain1_ref[...]).astype(jnp.bfloat16)
     hid[x] = own
-    down_y_end()
     halves = [pl.ds(i * (SUB // 2), SUB // 2) for i in (0, 1)]
     for n, half in enumerate(halves):
-        for i, d in enumerate((f, -f)):
-            send(hid.at[x, half, :], hid.at[x, half, :], hid_rcv.at[2 * i + n], dev(dx=d))
-    up_z_step(4)
-    arrived(wdn.at[:, y, 1 - c], dndd_rcv.at[0])
-    for i, d in enumerate((-1, 1)):
-        arrived(wdn.at[:, at_y(d), 1 - c], dndd_rcv.at[1 + i])
-    arrived(wdn.at[:, at_y(2), 1 - c], dndd_rcv.at[3])
+        send(hid.at[x, half, :], hid.at[x, half, :], hid_rcv.at[n], dev(dx=f))
+    for g in range(5):
+        down_y_end(g)
+    down_over(3)
+    up_z_step(3)
+    for n, half in enumerate(halves):
+        send(hid.at[x, half, :], hid.at[x, half, :], hid_rcv.at[2 + n], dev(dx=-f))
+    down_here()
     for i in range(NZ):
         wdnt[:, 256 * i : 256 * i + 256] = wdn[i].reshape(256, 1024).T
+    for n, half in enumerate(halves):
+        blk = hid.at[at_x(-f), half, :]
+        arrived(blk, hid_rcv.at[n])
+        send(blk, blk, hid_rcv.at[4 + n], dev(dx=f))
+    up_z_step(4)
     arrived(wup.at[z, :, 1 - c], updd_rcv.at[0])
     for d in (1, 2, 3):
         for i, s in enumerate((-1, 1)):
@@ -461,10 +487,6 @@
         return total
 
     post = mixer(own) + ALPHA * own.astype(jnp.float32)
-    for n, half in enumerate(halves):
-        blk = hid.at[at_x(-f), half, :]
-        arrived(blk, hid_rcv.at[n])
-        send(blk, blk, hid_rcv.at[4 + n], dev(dx=f))
     for n, half in enumerate(halves):
         arrived(hid.at[at_x(f), half, :], hid_rcv.at[2 + n])
     both = mixer(jnp.concatenate([hid[at_x(-f)], hid[at_x(f)]], axis=0))
@@ -540,7 +562,7 @@
             pltpu.VMEM((4, 128, 256), bf),
             pltpu.VMEM((8, 1, 256), f32),
             pltpu.VMEM((1024, 2048), bf),
-            dma((128,)),
+            dma((160,)),
             dma((12,)),
             dma((8, 2)),
             dma((4, 2)),
@@ -552,7 +574,7 @@
             dma((7,)),
             dma((8,)),
             dma((7,)),
-            dma((3,)),
+            dma((24,)),
             dma((4,)),
             dma((3,)),
             dma((3,)),

time: 91 us -> 88.2 us (0.969)
  Pallas kernels: 88.8 us -> 86.4 us
    pallas_call x1, Pallas kernels: 88.8 us -> 86.4 us  [local(): pl.pallas_call(layer_kernel, out_shape=jax.ShapeDtypeStruct((SUB, 2048),...]
where the time goes in v4:
time: 88.2 us; the launch traced here: 88.1 us
  Pallas kernels  86.4 us (98%)
  local copies, waits for them, and re-layouts  1.67 us (2%)
    pallas_call x1, Pallas kernels, local(): pl.pallas_call(layer_kernel, out_shape=jax.ShapeDtypeStruct((SUB, 2048),...  86.4 us

profile of v4, /device:TPU:2, one launch (start us, length us, event | category | flops | bytes accessed | tf_op | source)
XLA Modules:
  0.0 88.1 jit_solution(8791339120601331793)
XLA Ops:
  0.0 86.4 %layer.1 = bf16[64,2048]{1,0:T(8,128)(2,1)} custom-call(f32[2]{0:T(128)} %lam_ref.1, bf16[256,128]{1,0:T(8,128)(2,1)} %q1_hbm.1, bf16[256,128]{1,0:T(8,128)(2,1)} %q2_hbm.1, bf16[256,128]{1,0:T(8,128)(2,1)} %k1_hbm.1, bf16[256,128]{1,0:T(8,128)(2,1)} %k2_hbm.1, bf16[256,256]{1,0:T(8,128)(2,1)} %v_hbm.1, f32[1,128]{1,0:T(1,128)} %bitcast.7, ...), custom_call_target="tpu_custom_call" | custom-call | flops 20000000000 | bytes 4000000 | tf_op jit(solution)/shard_map/layer/pallas_call | solution.py:523
  86.4 1.7 %copy.15 = bf16[64,2048]{1,0:T(8,128)(2,1)} copy(bf16[64,2048]{1,0:T(8,128)(2,1)} %layer.1) | data formatting | bytes 524288

commit v5 on v4

--- a/solution.py
+++ b/solution.py
@@ -312,15 +312,17 @@
 
     def finish(qs, place):
         for i in range(4):
-            osend[place, i] = (acc[qs * 4 + i] / lbuf[qs * 4 + i]).astype(jnp.bfloat16)
-        for i in range(4):
             ssend[place, i] = mbuf[qs * 4 + i]
             ssend[place, 4 + i] = lbuf[qs * 4 + i]
+        for i in range(4):
+            osend[place, i] = (acc[qs * 4 + i] / lbuf[qs * 4 + i]).astype(jnp.bfloat16)
 
     def opposite_out():
         finish(3, 0)
-        send(osend.at[0], orelay, or_rcv.at[0], dev(dy=f))
-        send(ssend.at[0], srelay, or_rcv.at[1], dev(dy=f))
+        send(ssend.at[0], srelay, or_rcv.at[2], dev(dy=f))
+        for cc in (0, 1):
+            part = pl.ds(2 * cc, 2)
+            send(osend.at[0, part], orelay.at[part], or_rcv.at[cc], dev(dy=f))
 
     def direct_out():
         finish(q_direct, 1)
@@ -328,20 +330,25 @@
         send(ssend.at[1], srecv.at[0], s_rcv.at[0], dev(dy=-f))
 
     def merged_out():
-        arrived(orelay, or_rcv.at[0])
-        arrived(srelay, or_rcv.at[1])
+        arrived(srelay, or_rcv.at[2])
+        shares = []
         for i in range(4):
             m, l = mbuf[q_merged * 4 + i], lbuf[q_merged * 4 + i]
             top = jnp.maximum(m, srelay[i])
             w, v = jnp.exp2(m - top), jnp.exp2(srelay[i] - top) * srelay[4 + i]
             total = l * w + v
-            osend[2, i] = (
-                acc[q_merged * 4 + i] * (w / total) + orelay[i].astype(jnp.float32) * (v / total)
-            ).astype(jnp.bfloat16)
             ssend[2, i] = top
             ssend[2, 4 + i] = total
-        send(osend.at[2], orecv.at[1], o_rcv.at[1], dev(dy=f))
+            shares.append((w / total, v / total))
         send(ssend.at[2], srecv.at[1], s_rcv.at[1], dev(dy=f))
+        for cc in (0, 1):
+            part = pl.ds(2 * cc, 2)
+            arrived(orelay.at[part], or_rcv.at[cc])
+            for i in (2 * cc, 2 * cc + 1):
+                osend[2, i] = (
+                    acc[q_merged * 4 + i] * shares[i][0] + orelay[i].astype(jnp.float32) * shares[i][1]
+                ).astype(jnp.bfloat16)
+            send(osend.at[2, part], orecv.at[1, part], o_rcv.at[1 + cc], dev(dy=f))
 
     arrived(qbuf.at[0, 1 - c], q_rcv.at[0, 1 - c])
     expand(0)
@@ -364,19 +371,19 @@
     down_z_step(2)
     down_y_start(2)
     process(0, 2, 3, 1)
+    up_y_on()
+    down_y_on(0)
     take_kv(3)
     take_kv(4)
-    up_y_on()
-    down_y_on(0)
     process(2, 1, 0, 4, then=(3, 0))
     down_z_step(3)
     down_y_start(3)
-    down_y_on(1)
-    up_y_end()
     process(3, 1, 0, 4, ready=True)
     take_kv(5)
     take_kv(6)
+    up_y_end()
     up_z_start()
+    down_y_on(1)
     down_y_on(2)
     out_weight_on()
     process(4, 1, 0, 4, then=(5, 3))
@@ -398,13 +405,14 @@
     merged_out()
     down_y_on(4)
 
+    arrived(orecv.at[0], o_rcv.at[0])
     for j in (0, 1):
-        arrived(orecv.at[j], o_rcv.at[j])
         arrived(srecv.at[j], s_rcv.at[j])
     locals_[5].wait()
     lam = lam_ref[c]
     gain = gain_ref[...] * 0.8
     for cc in (0, 1):
+        arrived(orecv.at[1, pl.ds(2 * cc, 2)], o_rcv.at[1 + cc])
         maps = []
         for mp in (0, 1):
             i = 2 * cc + mp
@@ -581,7 +589,7 @@
             dma((6,)),
             dma((6,)),
             dma((4,)),
-            dma((2,)),
+            dma((3,)),
         ],
         compiler_params=pltpu.CompilerParams(
             collective_id=0, has_side_effects=True, vmem_limit_bytes=56 * 1024 * 1024

time: 88.2 us -> 88.3 us (level)
  no operation moved by 1% of the time
where the time goes in v5:
time: 88.3 us; the launch traced here: 88.1 us
  Pallas kernels  86.4 us (98%)
  local copies, waits for them, and re-layouts  1.67 us (2%)
    pallas_call x1, Pallas kernels, local(): pl.pallas_call(layer_kernel, out_shape=jax.ShapeDtypeStruct((SUB, 2048),...  86.4 us

profile of v5, /device:TPU:2, one launch (start us, length us, event | category | flops | bytes accessed | tf_op | source)
XLA Modules:
  0.0 88.1 jit_solution(3261238985367966981)
XLA Ops:
  0.0 86.4 %layer.1 = bf16[64,2048]{1,0:T(8,128)(2,1)} custom-call(f32[2]{0:T(128)} %lam_ref.1, bf16[256,128]{1,0:T(8,128)(2,1)} %q1_hbm.1, bf16[256,128]{1,0:T(8,128)(2,1)} %q2_hbm.1, bf16[256,128]{1,0:T(8,128)(2,1)} %k1_hbm.1, bf16[256,128]{1,0:T(8,128)(2,1)} %k2_hbm.1, bf16[256,256]{1,0:T(8,128)(2,1)} %v_hbm.1, f32[1,128]{1,0:T(1,128)} %bitcast.7, ...), custom_call_target="tpu_custom_call" | custom-call | flops 20000000000 | bytes 4000000 | tf_op jit(solution)/shard_map/layer/pallas_call | solution.py:531
  86.4 1.7 %copy.15 = bf16[64,2048]{1,0:T(8,128)(2,1)} copy(bf16[64,2048]{1,0:T(8,128)(2,1)} %layer.1) | data formatting | bytes 524288

commit v6 on v4

--- a/solution.py
+++ b/solution.py
@@ -25,9 +25,9 @@
 
 
 def layer_kernel(
-    lam_ref, q1_hbm, q2_hbm, k1_hbm, k2_hbm, v_hbm, hgain_hbm, stream_hbm, ow_hbm, gain1_hbm, up_hbm, down_hbm, gain2_hbm,
+    lam_ref, q1_hbm, q2_hbm, k1_hbm, k2_hbm, v_hbm, hgain_hbm, stream_hbm, ow_hbm, gain1_hbm, up_hbm, down_hbm,
     out_ref,
-    q1_ref, q2_ref, k1_ref, k2_ref, v_ref, gain_ref, gain1_ref, gain2_ref,
+    q1_ref, q2_ref, k1_ref, k2_ref, v_ref, gain_ref, gain1_ref,
     kvsrc, qsrc, kvbuf, qbuf, acc, mbuf, lbuf, qexp, sbuf, topbuf, osend, ssend, orecv, srecv, attown, attbuf, strbuf,
     wout, wup, wdn, hid, psend, precv, pown, prelay, orelay, srelay, wdnt,
     snd, loc, kv_rcv, q_rcv, o_rcv, s_rcv, str_rcv, att_rcv,
@@ -68,6 +68,14 @@
             src_ref=dst, dst_ref=dst, send_sem=snd.at[0], recv_sem=rcv, device_id=sibling, device_id_type=MESH
         ).wait_recv()
 
+    barrier = pltpu.get_barrier_semaphore()
+    partners = [sibling, dev(dy=2)]
+    for core in (0, 1):
+        partners += [dev(dz=1, core=core), dev(dz=-1, core=core), dev(dy=1, core=core), dev(dy=-1, core=core)]
+        partners += [dev(dx=d, core=core) for d in (1, 2, 3)]
+    for p in partners:
+        pl.semaphore_signal(barrier, inc=1, device_id=p, device_id_type=MESH)
+
     mine = pl.ds(pl.multiple_of(x * SUB, SUB), SUB)
 
     def ow_rows(d, half):
@@ -75,7 +83,7 @@
 
     local_pairs = [
         (q1_hbm, q1_ref), (q2_hbm, q2_ref), (k1_hbm, k1_ref), (k2_hbm, k2_ref), (v_hbm, v_ref),
-        (hgain_hbm, gain_ref), (gain1_hbm, gain1_ref), (gain2_hbm, gain2_ref),
+        (hgain_hbm, gain_ref), (gain1_hbm, gain1_ref),
         (stream_hbm.at[mine, :], strbuf.at[x]),
         (up_hbm, wup.at[z, y, c]), (down_hbm, wdn.at[z, y, c]),
         (ow_hbm, wout.at[pl.ds(pl.multiple_of(x * 256, 256), 256), :]),
@@ -84,22 +92,6 @@
     for cp in locals_:
         cp.start()
 
-    barrier = pltpu.get_barrier_semaphore()
-    partners = [sibling, dev(dy=2)]
-    for core in (0, 1):
-        partners += [dev(dz=1, core=core), dev(dz=-1, core=core), dev(dy=1, core=core), dev(dy=-1, core=core)]
-        partners += [dev(dx=d, core=core) for d in (1, 2, 3)]
-    for p in partners:
-        pl.semaphore_signal(barrier, inc=1, device_id=p, device_id_type=MESH)
-
-    mbuf[...] = jnp.full(mbuf.shape, LOW, jnp.float32)
-    lbuf[...] = jnp.zeros(lbuf.shape, jnp.float32)
-
-    def clear(i, carry):
-        acc[i] = jnp.zeros(acc.shape[1:], jnp.float32)
-        return carry
-
-    lax.fori_loop(0, acc.shape[0], clear, 0)
     for cp in locals_[:5]:
         cp.wait()
 
@@ -119,12 +111,11 @@
         kvsrc[h, 384:512, :] = vt[128 * h : 128 * h + 128, 128:256]
     kvbuf[0, c] = kvsrc[c]
     qbuf[0, c] = qsrc[c]
-    for i in (9, 10, 11):
-        locals_[i].wait()
     pl.semaphore_wait(barrier, len(partners))
 
     send(qsrc.at[1 - c], qbuf.at[0, c], q_rcv.at[0, c], sibling)
     send(kvsrc.at[1 - c], kvbuf.at[0, c], kv_rcv.at[0, c], sibling)
+    locals_[9].wait()
     for i, d in enumerate((1, -1)):
         send(wdn.at[z, y, c], wdn.at[z, y, c], dnz_rcv.at[i], dev(dz=d))
     for h in (0, 1):
@@ -135,6 +126,8 @@
     for dx in (1, 2, 3):
         rows = pl.ds(pl.multiple_of(at_x(dx) * SUB, SUB), SUB)
         send(stream_hbm.at[rows, :], strbuf.at[x], str_rcv.at[dx - 1], dev(dx=dx))
+    locals_[8].wait()
+    locals_[10].wait()
     for i, d in enumerate((1, -1)):
         send(wout.at[ow_rows(0, c), :], wout.at[ow_rows(0, c), :], ow_rcv.at[i], dev(dx=d))
 
@@ -343,6 +336,14 @@
         send(osend.at[2], orecv.at[1], o_rcv.at[1], dev(dy=f))
         send(ssend.at[2], srecv.at[1], s_rcv.at[1], dev(dy=f))
 
+    mbuf[...] = jnp.full(mbuf.shape, LOW, jnp.float32)
+    lbuf[...] = jnp.zeros(lbuf.shape, jnp.float32)
+
+    def clear(i, carry):
+        acc[i] = jnp.zeros(acc.shape[1:], jnp.float32)
+        return carry
+
+    lax.fori_loop(0, acc.shape[0], clear, 0)
     arrived(qbuf.at[0, 1 - c], q_rcv.at[0, 1 - c])
     expand(0)
     arrived(kvbuf.at[0, 1 - c], kv_rcv.at[0, 1 - c])
@@ -438,7 +439,7 @@
     down_over(2)
     for i in range(3):
         arrived(wout.at[ow_rows((-1, 1, 2)[i], 1 - c), :], owdd_rcv.at[i])
-    for i in (6, 7, 8):
+    for i in (6, 7):
         locals_[i].wait()
     for dx in (1, 2, 3):
         arrived(strbuf.at[at_x(-dx)], str_rcv.at[dx - 1])
@@ -508,7 +509,7 @@
         arrived(precv.at[1, part, :], p_rcv.at[1 + i])
     for i in range(2):
         post = post + precv[i].astype(jnp.float32)
-    out_ref[...] = layer_norm(post, gain2_ref[...]).astype(jnp.bfloat16)
+    out_ref[...] = layer_norm(post, 1.0)
     for cp in started:
         cp.wait_send()
 
@@ -520,10 +521,10 @@
     bf, f32 = jnp.bfloat16, jnp.float32
     hbm = pl.BlockSpec(memory_space=pltpu.HBM)
     dma = pltpu.SemaphoreType.DMA
-    return pl.pallas_call(
+    normed = pl.pallas_call(
         layer_kernel,
-        out_shape=jax.ShapeDtypeStruct((SUB, 2048), bf),
-        in_specs=[pl.BlockSpec(memory_space=pltpu.SMEM)] + [hbm] * 12,
+        out_shape=jax.ShapeDtypeStruct((SUB, 2048), f32),
+        in_specs=[pl.BlockSpec(memory_space=pltpu.SMEM)] + [hbm] * 11,
         out_specs=pl.BlockSpec(memory_space=pltpu.VMEM),
         scratch_shapes=[
             pltpu.VMEM((256, 128), bf),
@@ -532,7 +533,6 @@
             pltpu.VMEM((256, 128), bf),
             pltpu.VMEM((256, 256), bf),
             pltpu.VMEM((1, 128), f32),
-            pltpu.VMEM((1, 2048), f32),
             pltpu.VMEM((1, 2048), f32),
             pltpu.VMEM((2, 512, 128), bf),
             pltpu.VMEM((2, 128, 256), bf),
@@ -590,8 +590,9 @@
         name="layer",
     )(
         mix_lambda, query_one, query_two, key_one, key_two, values, head_gain.reshape(1, 128), stream, out_weight,
-        first_gain.reshape(1, 2048), up_weight, down_weight.T, second_gain.reshape(1, 2048),
+        first_gain.reshape(1, 2048), up_weight, down_weight.T,
     )
+    return (normed * second_gain).astype(bf)
 
 
 def solution(mesh):

time: 88.2 us -> 88.7 us (level)
  other arithmetic: 0 us -> 1.78 us
  local copies, waits for them, and re-layouts: 1.67 us -> 0.01 us
    convert_element_type x0 -> x1, other arithmetic: none -> 1.78 us  [local(): return (normed * second_gain).astype(bf)]
    unnamed x1 -> x2, local copies, waits for them, and re-layouts: 1.67 us -> 0.01 us
where the time goes in v6:
time: 88.7 us; the launch traced here: 88.6 us
  Pallas kernels  86.8 us (98%)
  other arithmetic  1.78 us (2%)
    pallas_call x1, Pallas kernels, local(): pl.pallas_call(layer_kernel, out_shape=jax.ShapeDtypeStruct((SUB, 2048),...  86.8 us
    convert_element_type x1, other arithmetic, local(): return (normed * second_gain).astype(bf)  1.78 us

profile of v6, /device:TPU:2, one launch (start us, length us, event | category | flops | bytes accessed | tf_op | source)
XLA Modules:
  0.0 88.6 jit_solution(242990318397126055)
XLA Ops:
  0.0 0.0 copy-start
  0.0 86.8 %layer.1 = f32[64,2048]{1,0:T(8,128)} custom-call(f32[2]{0:T(128)} %lam_ref.1, bf16[256,128]{1,0:T(8,128)(2,1)} %q1_hbm.1, bf16[256,128]{1,0:T(8,128)(2,1)} %q2_hbm.1, bf16[256,128]{1,0:T(8,128)(2,1)} %k1_hbm.1, bf16[256,128]{1,0:T(8,128)(2,1)} %k2_hbm.1, bf16[256,256]{1,0:T(8,128)(2,1)} %v_hbm.1, f32[1,128]{1,0:T(1,128)} %bitcast.5, ...), custom_call_target="tpu_custom_call" | custom-call | flops 20000000000 | bytes 4000000 | tf_op jit(solution)/shard_map/layer/pallas_call | solution.py:524
  86.8 0.0 copy-done
  86.8 1.8 %multiply_convert_fusion = bf16[64,2048]{1,0:T(8,128)(2,1)} fusion(f32[64,2048]{1,0:T(8,128)} %layer.1, f32[2048]{0:T(1024)S(1)} %copy-done), kind=kLoop, calls=%fused_computation | loop fusion | flops 262144 | bytes 794624 | tf_op jit(solution)/shard_map/convert_element_type | solution.py:595
Async XLA Ops:
  0.0 86.8 %copy-start = (f32[2048]{0:T(1024)S(1)}, f32[2048]{0:T(1024)}, u32[]{:S(2)}) copy-start(f32[2048]{0:T(1024)} %param.25) | copy-start | bytes 24580
